TPU v7x, 512 devices: a whole 4x8x8 slice. The times are simulated.
512 devices in a mesh: sp: 64 (over z, y), tp: 8 (over x, core).
Axes of the slice: x: 4, y: 8, z: 8, core: 2. Of those that a mesh axis runs over, the one named last changes fastest.
Arguments:
- value_in: bfloat16 [23040, 2048], P('sp', 'tp'), may hold values from -240 to 240
- gate_in: bfloat16 [23040, 2048], P('sp', 'tp'), may hold values from -8 to 8
- taps: float32 [31, 2048], P(None, 'tp'), may hold values from -1 to 1
- norm_gain: float32 [2048], P('tp'), may hold values from 0.1 to 1.9
- norm_bias: float32 [2048], P('tp'), may hold values from -3 to 3
- proj_weight: bfloat16 [2048, 4096], P('tp', 'sp'), may hold values from -0.125 to 0.125
- out_grad: bfloat16 [23040, 4096], P('sp'), may hold values from -16 to 16
Outputs:
- value_grad: bfloat16 [23040, 2048], P('sp', 'tp')
- gate_grad: bfloat16 [23040, 2048], P('sp', 'tp')
- tap_grad: float32 [31, 2048], P(None, 'tp')
- gain_grad: float32 [2048], P('tp')
- bias_grad: float32 [2048], P('tp')
- weight_grad: float32 [2048, 4096], P('tp', 'sp')
All inputs are finite; a program needn't handle non-finite values.
Results may differ from a plain program's by a relative error of at most 0.0051.
Values may be sent and summed in bfloat16 or wider, within the bound.
A program may use at most 64 MiB of HBM per device.

v0:
```python
import functools

import jax
import jax.numpy as jnp
from jax import lax
from jax.sharding import Mesh
from jax.sharding import PartitionSpec as P

SP = ("sp_0", "sp_1")


def padded_2(cells, sides, width):
    for axis, dim in sides:
        count = lax.axis_size(axis)
        ends = count - 1
        head = lax.slice_in_dim(cells, 0, width, axis=dim)
        tail = lax.slice_in_dim(cells, cells.shape[dim] - width, cells.shape[dim], axis=dim)
        cells = jnp.concatenate(
            [
                lax.ppermute(tail, axis, [(i, (i + 1) % count) for i in range(ends)]),
                cells,
                lax.ppermute(head, axis, [((i + 1) % count, i) for i in range(ends)]),
            ],
            axis=dim,
        )
    return cells


def copy_for_each(value, axis):
    copies = jnp.broadcast_to(value, (lax.axis_size(axis), *value.shape))
    return lax.all_to_all(copies, axis, split_axis=0, concat_axis=0, tiled=True)


def of_everyone(value, axis):
    everything = copy_for_each(value, axis)
    return jnp.sum(everything, axis=0)


def together(arrays, axis):
    flat, at, finished = (jnp.concatenate([a.reshape(-1) for a in arrays]), 0, [])
    subtotal = of_everyone(flat, axis)
    for a in arrays:
        finished.append(subtotal[at : at + a.size].reshape(a.shape))
        at += a.size
    return tuple(finished)


def in_order(tiles, dim):
    tiles = jnp.moveaxis(tiles, 0, dim)
    lengths = tiles.shape
    return tiles.reshape(*lengths[:dim], lengths[dim] * lengths[dim + 1], *lengths[dim + 2 :])


def stacked_from(value, axes, order):
    tiles = value[None]
    for k in order:
        tiles = lax.all_gather(tiles, axes[k], axis=0, tiled=True)
    held = [lax.axis_size(axes[k]) for k in reversed(order)]
    tiles = tiles.reshape(*held, *value.shape)
    turned = sorted(range(len(order)), key=lambda place: order[len(order) - 1 - place])
    return tiles.transpose(*turned, *range(len(order), tiles.ndim)).reshape(-1, *value.shape)


def gather_axes(value, axes, order, dim):
    return in_order(stacked_from(value, axes, order), dim)


def passed_along(block, axis, distance):
    devices = range(lax.axis_size(axis))
    route = [(i - distance, i) for i in devices if i - distance in devices]
    return lax.ppermute(block, axis, route)


def by_axis(value, axes):
    return functools.reduce(lax.psum, axes, value)


def summed_rows(subtotal, axes):
    for axis in axes:
        subtotal = lax.psum_scatter(subtotal, axis, scatter_dimension=0, tiled=True)
    return subtotal


def on_device(value_in, gate_in, taps, norm_gain, norm_bias, proj_weight, out_grad):
    f32 = jnp.float32
    rows = value_in.shape[0]
    local_width = value_in.shape[1]
    span = taps.shape[0]
    half = span // 2
    width_all = local_width * lax.axis_size("tp")
    gate_sig = jax.nn.sigmoid(gate_in.astype(f32))
    value_f = value_in.astype(f32)
    mixed = (value_f * gate_sig).astype(jnp.bfloat16)
    padded = padded_2(mixed, ((SP, 0),), half).astype(f32)
    conv = jnp.zeros((rows, local_width), f32)
    for k in range(span):
        conv = conv + taps[k] * padded[k : k + rows]
    total, squares = together((jnp.sum(conv, axis=1), jnp.sum(conv * conv, axis=1)), "tp")
    mean = total / width_all
    centred = conv - mean[:, None]
    spread = squares / width_all - mean * mean
    inv = lax.rsqrt(spread + 1e-06)
    normed = centred * inv[:, None]
    pre = normed * norm_gain + norm_bias
    act = jax.nn.silu(pre).astype(jnp.bfloat16)
    columns = out_grad
    act_grad = lax.dot_general(
        columns,
        gather_axes(proj_weight, SP, (0, 1), 1),
        (((1,), (1,)), ((), ())),
        preferred_element_type=f32,
    )
    sig_pre = jax.nn.sigmoid(pre)
    pre_grad = act_grad * sig_pre * (1.0 + pre * (1.0 - sig_pre))
    normed_grad = pre_grad * norm_gain
    first, second = together(
        (jnp.sum(normed_grad, axis=1), jnp.sum(normed_grad * normed, axis=1)), "tp"
    )
    conv_grad = inv[:, None] * (
        normed_grad - first[:, None] / width_all - normed * second[:, None] / width_all
    )
    local_pad = jnp.pad(conv_grad, ((2 * half, 2 * half), (0, 0)))
    spread_out = jnp.zeros((rows + 2 * half, local_width), f32)
    for k in range(span):
        spread_out = spread_out + taps[k] * local_pad[2 * half - k : 2 * half - k + rows + 2 * half]
    own_part = spread_out[half : half + rows]
    from_left = passed_along(spread_out[rows + half :], SP, 1)
    from_right = passed_along(spread_out[:half], SP, -1)
    mixed_grad = own_part.at[:half].add(from_left).at[rows - half :].add(from_right)
    tap_local = jnp.stack([jnp.sum(conv_grad * padded[k : k + rows], axis=0) for k in range(span)])
    gain_local = jnp.sum(pre_grad * normed, axis=0)
    bias_local = jnp.sum(pre_grad, axis=0)
    tap_grad, gain_grad, bias_grad = (
        by_axis(tap_local, SP),
        by_axis(gain_local, SP),
        by_axis(bias_local, SP),
    )
    value_grad = (mixed_grad * gate_sig).astype(jnp.bfloat16)
    gate_grad = (mixed_grad * value_f * gate_sig * (1.0 - gate_sig)).astype(jnp.bfloat16)
    columns = out_grad
    summed = summed_rows(
        lax.dot_general(columns, act, (((0,), (0,)), ((), ())), preferred_element_type=f32), SP
    )
    weight_grad = jnp.transpose(summed)
    return (value_grad, gate_grad, tap_grad, gain_grad, bias_grad, weight_grad)


def solution(mesh):
    finer = Mesh(mesh.devices.reshape(8, 8, mesh.shape["tp"]), ("sp_0", "sp_1", "tp"))
    in_specs = (P(SP, "tp"), P(SP, "tp"), P(None, "tp"), P("tp"), P("tp"), P("tp", SP), P(SP, None))
    out_specs = (P(SP, "tp"), P(SP, "tp"), P(None, "tp"), P("tp"), P("tp"), P("tp", SP))
    return jax.shard_map(
        on_device, mesh=finer, in_specs=in_specs, out_specs=out_specs, check_vma=False
    )
```

profile of v0, /device:TPU:4, one launch (start us, length us, event | category | flops | bytes accessed | tf_op | source)
XLA Modules:
  0.0 201.0 jit_solution(267206037773052146)
XLA Ops:
  8.0 0.0 copy-start
  8.0 0.0 all-gather.3.cloned.1.call-start
  8.1 31.5 %all-gather = bf16[2048,64]{0,1:T(8,128)(2,1)S(1)} all-gather(bf16[256,64]{0,1:T(8,128)(2,1)} %param.16), channel_id=2, replica_groups=mesh['sp_0'=8,'sp_1'=8,'tp'=8] {'sp_0'}, dimensions={0}, use_global_device_ids=true | all-gather | bytes 294912 | tf_op jit(solution)/shard_map/all_gather | solution.py:57
  39.6 0.8 copy.41
  40.3 0.0 all-gather.3.cloned.1.call-update
  40.3 0.0 reduce-scatter.5.cloned.1.call-start
  40.4 1.1 fusion.62
  41.5 3.5 %collective-permute-start = (bf16[15,256]{1,0:T(8,128)(2,1)S(1)}, bf16[15,256]{1,0:T(8,128)(2,1)S(1)}, u32[]{:S(2)}, u32[]{:S(2)}) collective-permute-start(bf16[15,256]{1,0:T(8,128)(2,1)S(1)} %get-tuple-element.121), channel_id=1, source_target_pairs={{0,8},{8,16},{16,24},{24,32},{32,40},{40,48},{48,56},{56,64},{64,7... | collective-permute-start | bytes 23048 | tf_op jit(solution)/shard_map/ppermute | solution.py:20
  45.0 1.3 collective-permute-start.1
  46.3 1.0 fusion.75
  47.4 1.0 fusion.76
  48.3 0.0 collective-permute-done
  48.3 2.2 %collective-permute-done.1 = bf16[15,256]{1,0:T(8,128)(2,1)S(1)} collective-permute-done((bf16[15,256]{1,0:T(8,128)(2,1)S(1)}, bf16[15,256]{1,0:T(8,128)(2,1)S(1)}, u32[]{:S(2)}, u32[]{:S(2)}) %collective-permute-start.1) | collective-permute-done | bytes 7712 | tf_op jit(solution)/shard_map/ppermute | solution.py:22
  50.6 0.0 copy-start.5
  50.6 0.0 copy-start.6
  50.6 2.2 %fusion.72 = (f32[360]{0:T(512)S(1)}, f32[360]{0:T(512)S(1)}, f32[360,256]{1,0:T(8,128)}) fusion(f32[390,256]{1,0:T(8,128)S(1)} %maximum_convert_fusion, f32[256]{0:T(256)S(1)} %bitcast.144, f32[256]{0:T(256)S(1)} %bitcast.146, f32[256]{0:T(256)S(1)} %bitcast.88, f32[256]{0:T(256)S(1)} %bitcast.90, f32[256]{0:T(256)S(1)} %bitcast.92, f32[256]{0:T(256)S(1)} %bitcast.94, ...), kind=kLoop, calls=%fused_computation.158 | loop fusion | flops 5897520 | bytes 11831104 | tf_op jit(solution)/shard_map/reduce_sum | solution.py:98
  52.8 0.1 pad_maximum_fusion
  52.9 7.6 %all_to_all.12 = f32[8,1,720]{2,1,0:T(1,128)S(1)} all-to-all(f32[8,1,720]{2,1,0:T(1,128)S(1)} %broadcast_in_dim.6), channel_id=1, replica_groups=mesh['sp_0'=8,'sp_1'=8,'tp'=8] {'tp'}, dimensions={0} | all-to-all | bytes 46080 | tf_op jit(solution)/shard_map/all_to_all | solution.py:31
  60.5 0.1 add_rsqrt_fusion
  60.6 0.0 copy-done
  60.6 0.0 copy-done.5
  60.6 0.0 copy-done.6
  60.6 4.4 %convolution_bitcast_fusion = f32[4096,256]{0,1:T(8,128)} fusion(bf16[360,4096]{1,0:T(8,128)(2,1)S(1)} %copy-done, f32[360,256]{1,0:T(8,128)} %get-tuple-element.116, f32[256]{0:T(256)S(1)} %copy-done.6, f32[256]{0:T(256)S(1)} %copy-done.5, f32[360]{0:T(512)S(1)} %get-tuple-element.157, f32[360]{0:T(512)S(1)} %get-tuple-element.156), kind=kOutput, calls=%fused_computation | convolution fusion | flops 755804160 | bytes 7516992 | tf_op jit(solution)/shard_map/dot_general | solution.py:142
  65.0 0.0 reduce-scatter.5.cloned.1.call-update
  65.0 0.0 reduce-scatter.7.cloned.1.call-start
  65.1 24.0 %all-gather.3.cloned.1.call-done = bf16[64,256,64]{1,0,2:T(8,128)(2,1)} async-done(((bf16[8,256,64]{1,0,2:T(8,128)(2,1)}), bf16[64,256,64]{1,0,2:T(8,128)(2,1)}) %all-gather.3.cloned.1.call-update) | async-done | bytes 2097168 | tf_op jit(solution)/shard_map/all_gather | solution.py:57
  89.0 0.0 copy-start.1
  89.0 2.8 %copy.28 = bf16[8,8,256,64]{2,3,1,0:T(8,128)(2,1)S(1)} copy(bf16[8,8,256,64]{2,0,1,3:T(8,128)(2,1)} %bitcast.82) | data formatting | bytes 4194304 | tf_op jit(solution)/shard_map/transpose | solution.py:61
  91.9 0.0 copy-done.1
  91.9 2.4 %multiply_reduce_fusion = (f32[256]{0:T(256)}, f32[360]{0:T(512)S(1)}, f32[360]{0:T(512)S(1)}, f32[256]{0:T(256)}, f32[360,256]{1,0:T(8,128)}) fusion(f32[360,256]{1,0:T(8,128)S(1)} %copy-done.1, f32[360]{0:T(512)S(1)} %get-tuple-element.157, f32[360]{0:T(512)S(1)} %get-tuple-element.156, f32[256]{0:T(256)S(1)} %copy-done.5, f32[256]{0:T(256)S(1)} %copy-done.6, ...), kind=kOutput, calls=%fused_computation.102 | convolution fusion | flops 756724480 | bytes 5793408 | tf_op jit(solution)/shard_map/dot_general | solution.py:107
  94.3 0.1 pad_maximum_fusion.1
  94.4 7.6 %all_to_all.13 = f32[8,1,720]{2,1,0:T(1,128)S(1)} all-to-all(f32[8,1,720]{2,1,0:T(1,128)S(1)} %broadcast_in_dim.8), channel_id=1, replica_groups=mesh['sp_0'=8,'sp_1'=8,'tp'=8] {'tp'}, dimensions={0} | all-to-all | bytes 46080 | tf_op jit(solution)/shard_map/all_to_all | solution.py:31
  102.0 0.1 slice_multiply_fusion
  102.0 2.6 %multiply_reduce_fusion.1 = (f32[256]{0:T(256)S(1)}, f32[256]{0:T(256)}, f32[256]{0:T(256)}, f32[256]{0:T(256)}, f32[256]{0:T(256)}, /*index=5*/f32[256]{0:T(256...) fusion(f32[390,256]{1,0:T(8,128)S(1)} %maximum_convert_fusion, ...), kind=kLoop, calls=%fused_computation.103 | loop fusion | flops 4050432 | bytes 7766656 | tf_op jit(solution)/shard_map/reduce_sum | solution.py:130
  104.6 0.0 copy-start.2
  104.6 0.7 copy-done.2
  105.3 1.2 fusion.55
  106.6 0.0 copy-start.3
  106.6 0.7 copy-done.3
  107.3 0.6 fusion.73
  107.9 1.3 collective-permute-start.3
  109.2 5.1 %collective-permute-start.2 = (f32[15,256]{1,0:T(8,128)}, f32[15,256]{1,0:T(8,128)}, u32[]{:S(2)}, u32[]{:S(2)}) collective-permute-start(f32[15,256]{1,0:T(8,128)} %get-tuple-element.120), channel_id=1, source_target_pairs={{0,8},{8,16},{16,24},{24,32},{32,40},{40,48},{48,56},{56,64},{64,7... | collective-permute-start | bytes 46088 | tf_op jit(solution)/shard_map/ppermute | solution.py:71
  114.4 8.1 %reduce-scatter.5.cloned.1.call-done = f32[512,256]{0,1:T(8,128)} async-done(((f32[4096,256]{0,1:T(8,128)}), f32[512,256]{0,1:T(8,128)}) %reduce-scatter.5.cloned.1.call-update) | async-done | bytes 524304 | tf_op jit(solution)/shard_map/reduce_scatter | solution.py:80
  122.4 2.0 %copy.32 = f32[512,256]{1,0:T(8,128)} copy(f32[512,256]{0,1:T(8,128)} %reduce-scatter.5.cloned.1.call-done) | data formatting | bytes 1048576
  124.5 0.0 reduce-scatter.7.cloned.1.call-update
  124.5 0.0 copy-start.4
  124.5 2.2 %multiply_reduce_fusion.19 = (f32[256]{0:T(256)}, f32[256]{0:T(256)}, f32[256]{0:T(256)}, f32[256]{0:T(256)}, f32[256]{0:T(256)}, /*index=5*/f32[256]{0:T(256)},...) fusion(f32[360,256]{1,0:T(8,128)} %copy-done.2, ...), kind=kLoop, calls=%fused_computation.121 | loop fusion | flops 2392832 | bytes 5174272 | tf_op jit(solution)/shard_map/reduce_sum | solution.py:130
  126.7 2.9 %stack.127 = f32[31,256]{1,0:T(8,128)S(1)} concatenate(f32[1,256]{1,0:T(1,128)} %bitcast.178, f32[1,256]{1,0:T(1,128)} %bitcast.177, f32[1,256]{1,0:T(1,128)} %bitcast.176, f32[1,256]{1,0:T(1,128)} %bitcast.175, f32[1,256]{1,0:T(1,128)} %bitcast.174, f32[1,256]{1,0:T(1,128)} %bitcast.173, f32[1,256]{1,0:T(1,128)} %bitcast.172, f32[1,256]{1,0:T(1,128)} %bitcast.171, ...), dimensions={0} | concatenate | bytes 63488 | tf_op jit(solution)/shard_map/stack | solution.py:130
  129.5 29.3 %all-reduce.2 = (f32[31,256]{1,0:T(8,128)S(1)}, f32[256]{0:T(256)S(1)}, f32[256]{0:T(256)S(1)}) all-reduce(f32[31,256]{1,0:T(8,128)S(1)} %stack.127, f32[256]{0:T(256)} %get-tuple-element.103, f32[256]{0:T(256)} %get-tuple-element.106), channel_id=1, replica_groups=mesh['sp_0'=8,'sp_1'=8,'tp'=8] {'sp_0'}, use_global_device_ids=true, to_apply=%region_37.38 | all-reduce | flops 8448 | bytes 67584 | tf_op jit(solution)/shard_map/psum | solution.py:75
  158.8 30.7 %all-reduce.1 = (f32[31,256]{1,0:T(8,128)}, f32[256]{0:T(256)}, f32[256]{0:T(256)}) all-reduce(f32[31,256]{1,0:T(8,128)S(1)} %get-tuple-element.112, f32[256]{0:T(256)S(1)} %get-tuple-element.113, f32[256]{0:T(256)S(1)} %get-tuple-element.114), channel_id=1, replica_groups=mesh['sp_0'=8,'sp_1'=8,'tp'=8] {'sp_1'}, use_global_device_ids=true, to_apply=%region_38.39 | all-reduce | flops 8448 | bytes 67584 | tf_op jit(solution)/shard_map/psum | solution.py:75
  189.5 1.0 slice.544
  190.5 0.0 collective-permute-done.2
  190.5 0.8 slice_add_fusion.1
  191.3 0.2 scatter-add.6
  191.5 0.0 collective-permute-done.3
  191.5 0.2 scatter-add.9
  191.7 0.0 copy-done.4
  191.7 1.8 fusion.65
  193.5 0.0 reduce-scatter.7.cloned.1.call-done
  (7 shorter events, 0.1 us)
Async XLA Ops:
  8.0 52.6 %copy-start = (bf16[360,4096]{1,0:T(8,128)(2,1)S(1)}, bf16[360,4096]{1,0:T(8,128)(2,1)}, u32[]{:S(2)}) copy-start(bf16[360,4096]{1,0:T(8,128)(2,1)} %param.17) | copy-start | bytes 8847364
  8.0 81.0 %all-gather.3.cloned.1.call-start = ((), (), s32[]{:S(2)}) async-start(), calls=%async_computation.4 | async-start | bytes 2359296 | tf_op jit(solution)/shard_map/all_gather | solution.py:57
  40.3 82.1 %reduce-scatter.5.cloned.1.call-start = ((), (), s32[]{:S(2)}) async-start(), calls=%async_computation.5 | async-start | bytes 4718592 | tf_op jit(solution)/shard_map/reduce_scatter | solution.py:80
  41.5 6.8 %collective-permute-start = (bf16[15,256]{1,0:T(8,128)(2,1)S(1)}, bf16[15,256]{1,0:T(8,128)(2,1)S(1)}, u32[]{:S(2)}, u32[]{:S(2)}) collective-permute-start(bf16[15,256]{1,0:T(8,128)(2,1)S(1)} %get-tuple-element.121), channel_id=1, source_target_pairs={{0,8},{8,16},{16,24},{24,32},{32,40},{40,48},{48,56},{56,64},{64,7... | collective-permute-start | bytes 23048 | tf_op jit(solution)/shard_map/ppermute | solution.py:20
  45.0 5.5 %collective-permute-start.1 = (bf16[15,256]{1,0:T(8,128)(2,1)S(1)}, bf16[15,256]{1,0:T(8,128)(2,1)S(1)}, u32[]{:S(2)}, u32[]{:S(2)}) collective-permute-start(bf16[15,256]{1,0:T(8,128)(2,1)S(1)} %get-tuple-element.122), channel_id=1, source_target_pairs={{8,0},{16,8},{24,16},{32,24},{40,32},{48,40},{56,48},{64,56},{72,6... | collective-permute-start | bytes 23048 | tf_op jit(solution)/shard_map/ppermute | solution.py:22
  50.6 10.0 %copy-start.5 = (f32[256]{0:T(256)S(1)}, f32[256]{0:T(256)}, u32[]{:S(2)}) copy-start(f32[256]{0:T(256)} %param.14) | copy-start | bytes 3076
  50.6 10.0 %copy-start.6 = (f32[256]{0:T(256)S(1)}, f32[256]{0:T(256)}, u32[]{:S(2)}) copy-start(f32[256]{0:T(256)} %param.15) | copy-start | bytes 3076
  65.0 128.5 %reduce-scatter.7.cloned.1.call-start = ((), (), s32[]{:S(2)}) async-start(), calls=%async_computation.6 | async-start | bytes 589824
  89.0 2.8 %copy-start.1 = (f32[360,256]{1,0:T(8,128)S(1)}, f32[360,256]{1,0:T(8,128)}, u32[]{:S(2)}) copy-start(f32[360,256]{1,0:T(8,128)} %get-tuple-element.116) | copy-start | bytes 1105924
  104.6 0.7 copy-start.2
  106.6 0.8 copy-start.3
  107.9 83.6 %collective-permute-start.3 = (f32[15,256]{1,0:T(8,128)}, f32[15,256]{1,0:T(8,128)S(1)}, u32[]{:S(2)}, u32[]{:S(2)}) collective-permute-start(f32[15,256]{1,0:T(8,128)} %get-tuple-element.119), channel_id=1, source_target_pairs={{8,0},{16,8},{24,16},{32,24},{40,32},{48,40},{56,48},{64,56},{72,6... | collective-permute-start | bytes 46088 | tf_op jit(solution)/shard_map/ppermute | solution.py:71
  109.2 81.3 %collective-permute-start.2 = (f32[15,256]{1,0:T(8,128)}, f32[15,256]{1,0:T(8,128)}, u32[]{:S(2)}, u32[]{:S(2)}) collective-permute-start(f32[15,256]{1,0:T(8,128)} %get-tuple-element.120), channel_id=1, source_target_pairs={{0,8},{8,16},{16,24},{24,32},{32,40},{40,48},{48,56},{56,64},{64,7... | collective-permute-start | bytes 46088 | tf_op jit(solution)/shard_map/ppermute | solution.py:71
  124.5 67.2 %copy-start.4 = (bf16[360,256]{1,0:T(8,128)(2,1)S(1)}, bf16[360,256]{1,0:T(8,128)(2,1)}, u32[]{:S(2)}) copy-start(bf16[360,256]{1,0:T(8,128)(2,1)} %param.11) | copy-start | bytes 552964
Sparse Core Ops, SparseCore 0:
  40.5 48.5 all-gather.2
  124.6 38.2 reduce-scatter.6
Sparse Core Ops, SparseCore 1:
  65.1 57.3 reduce-scatter.4
where the time goes:
time: 202 us; the launch traced here: 201 us
  blocking collectives  107 us (53%)
  waiting for transfers between devices  34.3 us (17%)
  between operations  15.7 us (8%)
  local copies, waits for them, and re-layouts  14.1 us (7%)
  other arithmetic  12.2 us (6%)
  starting transfers between devices  11.3 us (6%)
  matrix products  6.77 us (3%)
    psum x2, blocking collectives, by_axis(): return functools.reduce(lax.psum, axes, value)  59.9 us
    all_gather x1, blocking collectives, stacked_from(): tiles = lax.all_gather(tiles, axes[k], axis=0, tiled=True)  31.5 us
    all_gather x1, waiting for transfers between devices, stacked_from(): tiles = lax.all_gather(tiles, axes[k], axis=0, tiled=True)  24 us
    all_to_all x2, blocking collectives, copy_for_each(): return lax.all_to_all(copies, axis, split_axis=0, concat_axis=0, tiled=True)  15.2 us
    reduce_scatter x1, waiting for transfers between devices, summed_rows(): subtotal = lax.psum_scatter(subtotal, axis, scatter_dimension=0, tiled=True)  8.09 us
    ppermute x2, starting transfers between devices, passed_along(): return lax.ppermute(block, axis, route)  6.43 us
    reduce_sum x2, other arithmetic, on_device(): jnp.sum(conv_grad * padded[k:k + rows], axis=0)  4.71 us
    dot_general x1, matrix products, on_device(): lax.dot_general(columns, act, (((0,), (0,)), ((), ())), preferred_element...  4.37 us
  transfers between devices with their start and end apart: 7, of which 3 were waited for; matrix products, arithmetic and copies ran while one was open for 15% of the time, Pallas kernels for 0%

commit v1 on v0

v1 whole, which is shorter than its diff:
```python
import functools

import jax
import jax.numpy as jnp
from jax import lax
from jax.experimental import pallas as pl
from jax.experimental.pallas import tpu as pltpu
from jax.sharding import Mesh
from jax.sharding import PartitionSpec as P

SP = ("sp_0", "sp_1")
MESH = pl.DeviceIdType.MESH
EPS = 1e-06
F32 = jnp.float32
BF16 = jnp.bfloat16
EDGE = 16


def kernel(
    cfg,
    v_hbm,
    g_hbm,
    taps_ref,
    gain_ref,
    bias_ref,
    w_ref,
    og_hbm,
    vg_ref,
    gg_ref,
    small_ref,
    wg_ref,
    v_s,
    g_s,
    og_s,
    vf_s,
    sig_s,
    mpad,
    conv_s,
    s1_s,
    s2_s,
    b1_s,
    b2_s,
    ib_s,
    act_f,
    act_s,
    ag_s,
    cgpad,
    tacc,
    halo_send,
    halo_recv,
    cg_recv,
    st_send,
    st_recv,
    wt_s,
    wgt_s,
    rs_s,
    rs_r,
    q_s,
    q_r,
    ar_s,
    ar_r,
    local_sem,
    halo_ss,
    halo_rs,
    st_ss,
    st_rs,
    a1_ss,
    a1_rs,
    a2_ss,
    a2_rs,
    r1_ss,
    r1_rs,
    r2_ss,
    r2_rs,
    ar_ss,
    ar_rs,
):
    nz, ny, nt, rows, width, span, chunk = cfg
    z, y, t = lax.axis_index("sp_0"), lax.axis_index("sp_1"), lax.axis_index("tp")
    count = nz * ny
    s = z * ny + y
    lanes = width // 2
    channels = width * nt
    steps = rows // chunk
    padded_rows = s1_s.shape[0]
    quarter = w_ref.shape[1] // 2

    def at(zz, yy, tt):
        return (zz, yy, tt)

    def along(h, phase, shift):
        on_y = (h == 0) == (phase == 1)
        if on_y:
            return at(z, lax.rem(y + shift + ny, ny), t)
        return at(lax.rem(z + shift + nz, nz), y, t)

    def size(h, phase):
        return ny if (h == 0) == (phase == 1) else nz

    def place(h, phase):
        return y if (h == 0) == (phase == 1) else z

    def cell(h, a, b):
        return (b, a) if h == 0 else (a, b)

    pending = []

    def send(src, dst, ssem, rsem, dev):
        copy = pltpu.make_async_remote_copy(
            src_ref=src, dst_ref=dst, send_sem=ssem, recv_sem=rsem, device_id=dev, device_id_type=MESH
        )
        copy.start()
        pending.append(copy)
        return copy

    load_v = pltpu.make_async_copy(v_hbm, v_s, local_sem.at[0])
    load_g = pltpu.make_async_copy(g_hbm, g_s, local_sem.at[1])
    load_og = pltpu.make_async_copy(og_hbm, og_s, local_sem.at[2])
    load_g.start()
    load_v.start()
    load_og.start()

    right = lax.rem(s + 1, count)
    left = lax.rem(s + count - 1, count)
    right_dev = at(right // ny, lax.rem(right, ny), t)
    left_dev = at(left // ny, lax.rem(left, ny), t)
    barrier = pltpu.get_barrier_semaphore()
    peers = [right_dev, left_dev]
    peers += [at(z, lax.rem(y + d, ny), t) for d in range(1, ny)]
    peers += [at(lax.rem(z + d, nz), y, t) for d in range(1, nz)]
    peers += [at(z, y, lax.rem(t + d, nt)) for d in range(1, nt)]
    for dev in peers:
        pl.semaphore_signal(barrier, inc=1, device_id=dev, device_id_type=MESH)

    n_col = w_ref.shape[1]
    eye = jnp.where(
        lax.broadcasted_iota(jnp.int32, (n_col, n_col), 0) == lax.broadcasted_iota(jnp.int32, (n_col, n_col), 1),
        jnp.ones((n_col, n_col), F32),
        jnp.zeros((n_col, n_col), F32),
    ).astype(BF16)
    turned = lax.dot_general(eye, w_ref[...], (((1,), (1,)), ((), ())), preferred_element_type=F32)
    wt_s[z, y] = turned.astype(BF16).reshape(2, quarter, width)

    load_g.wait()
    load_v.wait()
    sig = jax.nn.sigmoid(g_s[...].astype(F32))
    sig_s[...] = sig
    vf = v_s[...].astype(F32)
    vf_s[...] = vf
    mixed = (vf * sig).astype(BF16)
    halo_send[0] = mixed[rows - EDGE :]
    halo_send[1] = mixed[:EDGE]
    mpad[EDGE : EDGE + rows] = mixed.astype(F32)

    pl.semaphore_wait(barrier, len(peers))

    halo = [
        send(halo_send.at[0], halo_recv.at[0], halo_ss.at[0], halo_rs.at[0], right_dev),
        send(halo_send.at[1], halo_recv.at[1], halo_ss.at[1], halo_rs.at[1], left_dev),
    ]

    first, ring = {}, {}

    def near(d, n):
        return min(d, n - d)

    def ring_depth(h, d, sign):
        n = size(h, 2)
        even = d % 2 == 0
        return n // 2 if even == (sign > 0) else n // 2 - 1

    def forward(h, d, sign, k):
        a = lax.rem(place(h, 1) - d + size(h, 1), size(h, 1))
        n = size(h, 2)
        b = lax.rem(place(h, 2) - sign * (k - 1) + n, n)
        block = wt_s.at[(*cell(h, a, b), h)]
        i = 0 if sign > 0 else 1
        ring[h, d, sign, k] = send(
            block, block, a2_ss.at[h, d, i, k - 1], a2_rs.at[h, d, i, k - 1], along(h, 2, sign)
        )

    def gather_start():
        for h in range(2):
            for sign in (1, -1):
                if ring_depth(h, 0, sign) >= 1:
                    forward(h, 0, sign, 1)
        for h in range(2):
            n = size(h, 1)
            block = wt_s.at[(*cell(h, place(h, 1), place(h, 2)), h)]
            for d in sorted(range(1, n), key=lambda d: near(d, n)):
                first[h, d] = send(block, block, a1_ss.at[h, d], a1_rs.at[h, d], along(h, 1, d))

    def gather_round(r):
        for h in range(2):
            n = size(h, 1)
            for d in sorted(range(n), key=lambda d: near(d, n)):
                k = r - near(d, n) + 1
                if (d == 0 and k == 1) or k < 1 or k > size(h, 2) // 2 + 1:
                    continue
                if k == 1:
                    first[h, d].wait_recv()
                for sign in (1, -1):
                    depth = ring_depth(h, d, sign)
                    if 1 <= k - 1 <= depth:
                        ring[h, d, sign, k - 1].wait_recv()
                    if k <= depth:
                        forward(h, d, sign, k)

    rounds = max(size(h, 1) // 2 + size(h, 2) // 2 + 1 for h in range(2))
    gather_start()

    halo[0].wait_recv()
    halo[1].wait_recv()
    mpad[:EDGE] = jnp.where(s == 0, 0.0, halo_recv[0].astype(F32))
    mpad[EDGE + rows :] = jnp.where(s == count - 1, 0.0, halo_recv[1].astype(F32))

    def fold(x):
        return x[:, :lanes] + x[:, lanes:]

    def wide(x):
        return jnp.concatenate([x, x], axis=1)

    def conv_step(i, carry):
        base = i * chunk
        total = jnp.zeros((chunk, width), F32)
        for k in range(span):
            total = total + taps_ref[k : k + 1, :] * mpad[pl.ds(base + k + 1, chunk), :]
        conv_s[pl.ds(base, chunk), :] = total
        s1_s[pl.ds(base, chunk), :] = fold(total)
        s2_s[pl.ds(base, chunk), :] = fold(total * total)
        return carry

    for i in range(steps):
        conv_step(i, 0)

    def row_sums(which):
        a = jnp.sum(jnp.transpose(s1_s[...]), axis=0, keepdims=True)
        b = jnp.sum(jnp.transpose(s2_s[...]), axis=0, keepdims=True)
        both = jnp.concatenate([a, b], axis=0)
        st_send[which] = both
        copies = []
        for d in range(1, nt):
            copies.append(
                send(
                    st_send.at[which],
                    st_recv.at[which, d],
                    st_ss.at[which, d],
                    st_rs.at[which, d],
                    at(z, y, lax.rem(t + d, nt)),
                )
            )
        return copies

    def gathered_sums(which, copies):
        total = st_send[which]
        for d in range(1, nt):
            copies[d - 1].wait_recv()
            total = total + st_recv[which, d]
        return total / channels

    def down_rows(row):
        return jnp.transpose(jnp.broadcast_to(row, (lanes, padded_rows)))

    sums = row_sums(0)
    gather_round(0)
    gather_round(1)
    total = gathered_sums(0, sums)
    mean = total[0:1]
    inv = lax.rsqrt(total[1:2] - mean * mean + EPS)
    b1_s[...] = down_rows(mean)
    ib_s[...] = down_rows(inv)

    def act_step(i, carry):
        here = pl.ds(pl.multiple_of(i * chunk, 8), chunk)
        normed = (conv_s[here, :] - wide(b1_s[here, :])) * wide(ib_s[here, :])
        conv_s[here, :] = normed
        pre = normed * gain_ref[...] + bias_ref[...]
        act_f[here, :] = pre * jax.nn.sigmoid(pre)
        return carry

    lax.fori_loop(0, steps, act_step, 0)
    act_s[...] = act_f[...].astype(BF16)
    load_og.wait()
    gather_round(2)

    block_cols = ny * n_col

    def grad_step(i, carry):
        columns = pl.ds(pl.multiple_of(i * block_cols, 128), block_cols)
        part = lax.dot_general(
            og_s[:, columns], act_s[...], (((0,), (0,)), ((), ())), preferred_element_type=F32
        )
        wgt_s[i] = part.reshape(ny, 2, quarter, width)
        return carry

    lax.fori_loop(0, nz, grad_step, 0)

    hops, last = {}, {}

    def piece(h, c, p):
        n = size(h, 1) // 2
        if h == 0:
            return wgt_s[p, c * n : (c + 1) * n, 0]
        return wgt_s[c * n : (c + 1) * n, p, 1]

    def reduce_depth(h, c, sign):
        n = size(h, 2)
        return n // 2 if (c == 0) == (sign > 0) else n // 2 - 1

    def reduce_round(j):
        for h in range(2):
            n = size(h, 2)
            part = pl.ds(0, size(h, 1) // 2)
            for c in range(2):
                for i, sign in enumerate((1, -1)):
                    depth = reduce_depth(h, c, sign)
                    k = j - (n // 2 - depth)
                    if k < 1 or k > depth:
                        continue
                    dest = lax.rem(place(h, 2) + sign * (depth - k + 1) + n, n)
                    value = piece(h, c, dest)
                    if k > 1:
                        hops[h, c, sign, k - 1].wait_recv()
                        value = value + rs_r[h, c, i, k - 2, part].astype(F32)
                    rs_s[h, c, i, k - 1, part] = value.astype(BF16)
                    hops[h, c, sign, k] = send(
                        rs_s.at[h, c, i, k - 1, part],
                        rs_r.at[h, c, i, k - 1, part],
                        r1_ss.at[h, c, i, k - 1],
                        r1_rs.at[h, c, i, k - 1],
                        along(h, 2, sign),
                    )

    def reduce_finish():
        for h in range(2):
            n = size(h, 1) // 2
            for c in range(2):
                value = piece(h, c, place(h, 2))
                for i, sign in enumerate((1, -1)):
                    depth = reduce_depth(h, c, sign)
                    if depth:
                        hops[h, c, sign, depth].wait_recv()
                        value = value + rs_r[h, c, i, depth - 1, pl.ds(0, n)].astype(F32)
                if h == 0:
                    wgt_s[place(h, 2), c * n : (c + 1) * n, 0] = value
                else:
                    wgt_s[c * n : (c + 1) * n, place(h, 2), 1] = value
                q_s[h, c * n : (c + 1) * n] = value.astype(BF16)
            n = size(h, 1)
            for d in sorted(range(1, n), key=lambda d: near(d, n)):
                to = lax.rem(place(h, 1) + d, n)
                last[h, d] = send(
                    q_s.at[h, to], q_r.at[h, d], r2_ss.at[h, d], r2_rs.at[h, d], along(h, 1, d)
                )

    def reduce_end():
        for h in range(2):
            value = wgt_s[z, y, h]
            for d in range(1, size(h, 1)):
                last[h, d].wait_recv()
                value = value + q_r[h, d].astype(F32)
            wg_ref[h] = value

    gather_round(3)
    reduce_round(1)
    for r in range(4, rounds):
        gather_round(r)
    reduce_round(2)

    def product_step(i, carry):
        columns = pl.ds(pl.multiple_of(i * block_cols, 128), block_cols)
        part = jnp.dot(
            og_s[:, columns], wt_s[i].reshape(block_cols, width), preferred_element_type=F32
        )
        ag_s[...] = ag_s[...] + part
        return carry

    ag_s[...] = jnp.zeros_like(ag_s)
    lax.fori_loop(0, nz, product_step, 0)
    reduce_round(3)

    def pre_step(i, carry):
        gain_sum, bias_sum = carry
        here = pl.ds(pl.multiple_of(i * chunk, 8), chunk)
        normed = conv_s[here, :]
        pre = normed * gain_ref[...] + bias_ref[...]
        gate = jax.nn.sigmoid(pre)
        pre_grad = ag_s[here, :] * gate * (1.0 + pre * (1.0 - gate))
        gain_sum = gain_sum + jnp.sum((pre_grad * normed).reshape(chunk // 8, 8, width), axis=0)
        bias_sum = bias_sum + jnp.sum(pre_grad.reshape(chunk // 8, 8, width), axis=0)
        normed_grad = pre_grad * gain_ref[...]
        ag_s[here, :] = normed_grad
        s1_s[here, :] = fold(normed_grad)
        s2_s[here, :] = fold(normed_grad * normed)
        return gain_sum, bias_sum

    none = jnp.zeros((8, width), F32)
    gain_sum, bias_sum = lax.fori_loop(0, steps, pre_step, (none, none))
    gain_row = jnp.sum(gain_sum, axis=0, keepdims=True)
    bias_row = jnp.sum(bias_sum, axis=0, keepdims=True)
    sums = row_sums(1)
    reduce_round(4)
    total = gathered_sums(1, sums)
    b1_s[...] = down_rows(total[0:1])
    b2_s[...] = down_rows(total[1:2])

    def conv_grad_step(i, carry):
        base = pl.multiple_of(i * chunk, 8)
        here = pl.ds(base, chunk)
        value = wide(ib_s[here, :]) * (
            ag_s[here, :] - wide(b1_s[here, :]) - conv_s[here, :] * wide(b2_s[here, :])
        )
        cgpad[pl.ds(pl.multiple_of(base + EDGE, 8), chunk), :] = value
        return carry

    lax.fori_loop(0, steps, conv_grad_step, 0)
    back = [
        send(cgpad.at[pl.ds(rows, EDGE)], cg_recv.at[0], halo_ss.at[2], halo_rs.at[2], right_dev),
        send(cgpad.at[pl.ds(EDGE, EDGE)], cg_recv.at[1], halo_ss.at[3], halo_rs.at[3], left_dev),
    ]

    tacc[...] = jnp.zeros_like(tacc)

    def tap_step(i, carry):
        base = i * chunk
        value = cgpad[pl.ds(base + EDGE, chunk), :]
        for k in range(span):
            term = value * mpad[pl.ds(base + k + 1, chunk), :]
            tacc[k] = tacc[k] + jnp.sum(term.reshape(chunk // 8, 8, width), axis=0)
        return carry

    for i in range(steps):
        tap_step(i, 0)
    own_small = jnp.concatenate(
        [jnp.sum(tacc[...], axis=1), gain_row, bias_row, jnp.zeros((small_ref.shape[0] - span - 2, width), F32)],
        axis=0,
    )
    small_ref[...] = own_small

    def small_send(phase):
        copies = {}
        for h in range(2):
            ar_s[phase - 1, h] = small_ref[:, h * lanes : (h + 1) * lanes].astype(BF16)
        for h in range(2):
            n = size(h, phase)
            for d in sorted(range(1, n), key=lambda d: near(d, n)):
                copies[h, d] = send(
                    ar_s.at[phase - 1, h],
                    ar_r.at[phase - 1, h, d],
                    ar_ss.at[phase - 1, h, d],
                    ar_rs.at[phase - 1, h, d],
                    along(h, phase, d),
                )
        return copies

    def small_add(phase, copies):
        for h in range(2):
            value = ar_s[phase - 1, h].astype(F32)
            for d in range(1, size(h, phase)):
                copies[h, d].wait_recv()
                value = value + ar_r[phase - 1, h, d].astype(F32)
            small_ref[:, h * lanes : (h + 1) * lanes] = value

    small_1 = small_send(1)
    reduce_finish()

    back[0].wait_recv()
    back[1].wait_recv()
    cgpad[:EDGE] = jnp.where(s == 0, 0.0, cg_recv[0])
    cgpad[EDGE + rows :] = jnp.where(s == count - 1, 0.0, cg_recv[1])

    def mixed_step(i, carry):
        base = i * chunk
        total = jnp.zeros((chunk, width), F32)
        for k in range(span):
            total = total + taps_ref[k : k + 1, :] * cgpad[pl.ds(base + span - k, chunk), :]
        ag_s[pl.ds(base, chunk), :] = total
        return carry

    for i in range(steps):
        mixed_step(i, 0)
    small_add(1, small_1)
    small_2 = small_send(2)
    scaled = ag_s[...] * sig_s[...]
    vg_ref[...] = scaled.astype(BF16)
    gg_ref[...] = (scaled * vf_s[...] * (1.0 - sig_s[...])).astype(BF16)
    reduce_end()
    small_add(2, small_2)
    for copy in pending:
        copy.wait_send()


def on_device(sizes, value_in, gate_in, taps, norm_gain, norm_bias, proj_weight, out_grad):
    nz, ny, nt = sizes
    rows, width = value_in.shape
    span = taps.shape[0]
    n_col = proj_weight.shape[1]
    quarter = n_col // 2
    columns = out_grad.shape[1]
    lanes = width // 2
    chunk = next(c for c in (72, 24, 8) if rows % c == 0)
    padded_rows = (rows + 127) // 128 * 128
    small_rows = (span + 2 + 15) // 16 * 16
    n_max = max(nz, ny)
    n_half = n_max // 2
    dma = pltpu.SemaphoreType.DMA
    vmem = pl.BlockSpec(memory_space=pltpu.VMEM)
    anywhere = pl.BlockSpec(memory_space=pl.ANY)
    cfg = (nz, ny, nt, rows, width, span, chunk)
    vg, gg, small, wg = pl.pallas_call(
        functools.partial(kernel, cfg),
        out_shape=(
            jax.ShapeDtypeStruct((rows, width), BF16),
            jax.ShapeDtypeStruct((rows, width), BF16),
            jax.ShapeDtypeStruct((small_rows, width), F32),
            jax.ShapeDtypeStruct((2, quarter, width), F32),
        ),
        in_specs=[anywhere, anywhere, vmem, vmem, vmem, vmem, anywhere],
        out_specs=(vmem, vmem, vmem, vmem),
        scratch_shapes=[
            pltpu.VMEM((rows, width), BF16),
            pltpu.VMEM((rows, width), BF16),
            pltpu.VMEM((rows, columns), BF16),
            pltpu.VMEM((rows, width), F32),
            pltpu.VMEM((rows, width), F32),
            pltpu.VMEM((rows + 2 * EDGE, width), F32),
            pltpu.VMEM((rows, width), F32),
            pltpu.VMEM((padded_rows, lanes), F32),
            pltpu.VMEM((padded_rows, lanes), F32),
            pltpu.VMEM((padded_rows, lanes), F32),
            pltpu.VMEM((padded_rows, lanes), F32),
            pltpu.VMEM((padded_rows, lanes), F32),
            pltpu.VMEM((rows, width), F32),
            pltpu.VMEM((rows, width), BF16),
            pltpu.VMEM((rows, width), F32),
            pltpu.VMEM((rows + 2 * EDGE, width), F32),
            pltpu.VMEM((span, 8, width), F32),
            pltpu.VMEM((2, EDGE, width), BF16),
            pltpu.VMEM((2, EDGE, width), BF16),
            pltpu.VMEM((2, EDGE, width), F32),
            pltpu.VMEM((2, 2, padded_rows), F32),
            pltpu.VMEM((2, nt, 2, padded_rows), F32),
            pltpu.VMEM((nz, ny, 2, quarter, width), BF16),
            pltpu.VMEM((nz, ny, 2, quarter, width), F32),
            pltpu.VMEM((2, 2, 2, n_half, n_half, quarter, width), BF16),
            pltpu.VMEM((2, 2, 2, n_half, n_half, quarter, width), BF16),
            pltpu.VMEM((2, n_max, quarter, width), BF16),
            pltpu.VMEM((2, n_max, quarter, width), BF16),
            pltpu.VMEM((2, 2, small_rows, lanes), BF16),
            pltpu.VMEM((2, 2, n_max, small_rows, lanes), BF16),
            dma((3,)),
            dma((4,)),
            dma((4,)),
            dma((2, nt)),
            dma((2, nt)),
            dma((2, n_max)),
            dma((2, n_max)),
            dma((2, n_max, 2, n_half)),
            dma((2, n_max, 2, n_half)),
            dma((2, 2, 2, n_half)),
            dma((2, 2, 2, n_half)),
            dma((2, n_max)),
            dma((2, n_max)),
            dma((2, 2, n_max)),
            dma((2, 2, n_max)),
        ],
        compiler_params=pltpu.CompilerParams(
            collective_id=0, has_side_effects=True, vmem_limit_bytes=60 * 1024 * 1024
        ),
        name="step",
    )(value_in, gate_in, taps, norm_gain[None, :], norm_bias[None, :], proj_weight, out_grad)
    weight_grad = jnp.transpose(wg.reshape(n_col, width))
    return (vg, gg, small[:span], small[span], small[span + 1], weight_grad)


def solution(mesh):
    tp = mesh.shape["tp"]
    ny = 8 if mesh.shape["sp"] % 8 == 0 else 2
    nz = mesh.shape["sp"] // ny
    finer = Mesh(mesh.devices.reshape(nz, ny, tp), (*SP, "tp"))
    in_specs = (P(SP, "tp"), P(SP, "tp"), P(None, "tp"), P("tp"), P("tp"), P("tp", SP), P(SP, None))
    out_specs = (P(SP, "tp"), P(SP, "tp"), P(None, "tp"), P("tp"), P("tp"), P("tp", SP))
    return jax.shard_map(
        functools.partial(on_device, (nz, ny, tp)),
        mesh=finer,
        in_specs=in_specs,
        out_specs=out_specs,
        check_vma=False,
    )
```

time: 202 us -> 86.9 us (0.43)
  the two profiles are of different devices: /device:TPU:4 before, /device:TPU:8 now
where the time goes in v1:
time: 86.9 us; the launch traced here: 86.4 us
  Pallas kernels  77 us (89%)
  local copies, waits for them, and re-layouts  8.83 us (10%)
    pallas_call x1, Pallas kernels, on_device(): pl.pallas_call(functools.partial(kernel, cfg), out_shape=(jax.ShapeDtypeS...  77 us
    unnamed x4, local copies, waits for them, and re-layouts  6.18 us
    slice x2, local copies, waits for them, and re-layouts, on_device(): return (vg, gg, small[:span], small[span], small[span + 1], weight_grad)  2.66 us

profile of v1, /device:TPU:8, one launch (start us, length us, event | category | flops | bytes accessed | tf_op | source)
XLA Modules:
  0.0 86.4 jit_solution(15056671821521320662)
XLA Ops:
  0.6 1.5 %copy.13.w_ref = bf16[256,64]{1,0:T(8,128)(2,1)} copy(bf16[256,64]{0,1:T(8,128)(2,1)} %param.12) | data formatting | bytes 65536 | tf_op args[5]
  2.1 77.0 %step.1 = (bf16[360,256]{1,0:T(8,128)(2,1)}, bf16[360,256]{1,0:T(8,128)(2,1)}, f32[48,256]{1,0:T(8,128)}, f32[2,32,256]{2,1,0:T(8,128)}) custom-call(bf16[360,256]{1,0:T(8,128)(2,1)} %v_hbm.1, bf16[360,256]{1,0:T(8,128)(2,1)} %g_hbm.1, f32[31,256]{1,0:T(8,128)} %taps_ref.1, f32[1,256]{1,0:T(1,128)} %bitcast.8, f32[1,256]{1,0:T(1,128)} %bitcast.9, ...), custom_call_target="tpu_custom_call" | custom-call | tf_op jit(solution)/shard_map/step/pallas_call | solution.py:510
  79.1 1.3 %fusion = (f32[1,256]{1,0:T(1,128)}, f32[1,256]{1,0:T(1,128)}) fusion(f32[48,256]{1,0:T(8,128)} %get-tuple-element.12), kind=kLoop, calls=%fused_computation | loop fusion | bytes 4096 | tf_op jit(solution)/shard_map/slice | solution.py:573
  80.4 1.4 %slice.9 = f32[31,256]{1,0:T(8,128)} slice(f32[48,256]{1,0:T(8,128)} %get-tuple-element.12), slice={[0:31], [0:256]} | slice | bytes 63488 | tf_op jit(solution)/shard_map/slice | solution.py:573
  81.8 1.6 %copy.17 = bf16[360,256]{1,0:T(8,128)(2,1)} copy(bf16[360,256]{1,0:T(8,128)(2,1)} %get-tuple-element.22) | data formatting | bytes 368640
  83.4 1.6 %copy.18 = bf16[360,256]{1,0:T(8,128)(2,1)} copy(bf16[360,256]{1,0:T(8,128)(2,1)} %get-tuple-element.23) | data formatting | bytes 368640
  85.0 1.5 %copy.19 = f32[256,64]{0,1:T(8,128)} copy(f32[256,64]{0,1:T(8,128)} %bitcast.7) | data formatting | bytes 131072

commit v2 on v1

--- a/solution.py
+++ b/solution.py
@@ -20,10 +20,10 @@
     cfg,
     v_hbm,
     g_hbm,
-    taps_ref,
-    gain_ref,
-    bias_ref,
-    w_ref,
+    taps_hbm,
+    gain_hbm,
+    bias_hbm,
+    w_hbm,
     og_hbm,
     vg_ref,
     gg_ref,
@@ -32,6 +32,9 @@
     v_s,
     g_s,
     og_s,
+    taps_ref,
+    gain_ref,
+    bias_ref,
     vf_s,
     sig_s,
     mpad,
@@ -83,7 +86,8 @@
     channels = width * nt
     steps = rows // chunk
     padded_rows = s1_s.shape[0]
-    quarter = w_ref.shape[1] // 2
+    quarter = w_hbm.shape[1]
+    n_col = 2 * quarter
 
     def at(zz, yy, tt):
         return (zz, yy, tt)
@@ -116,9 +120,12 @@
     load_v = pltpu.make_async_copy(v_hbm, v_s, local_sem.at[0])
     load_g = pltpu.make_async_copy(g_hbm, g_s, local_sem.at[1])
     load_og = pltpu.make_async_copy(og_hbm, og_s, local_sem.at[2])
-    load_g.start()
-    load_v.start()
-    load_og.start()
+    load_w = pltpu.make_async_copy(w_hbm, wt_s.at[z, y], local_sem.at[3])
+    load_taps = pltpu.make_async_copy(taps_hbm, taps_ref, local_sem.at[4])
+    load_gain = pltpu.make_async_copy(gain_hbm, gain_ref, local_sem.at[5])
+    load_bias = pltpu.make_async_copy(bias_hbm, bias_ref, local_sem.at[6])
+    for load in (load_g, load_v, load_w, load_taps, load_gain, load_bias, load_og):
+        load.start()
 
     right = lax.rem(s + 1, count)
     left = lax.rem(s + count - 1, count)
@@ -132,15 +139,6 @@
     for dev in peers:
         pl.semaphore_signal(barrier, inc=1, device_id=dev, device_id_type=MESH)
 
-    n_col = w_ref.shape[1]
-    eye = jnp.where(
-        lax.broadcasted_iota(jnp.int32, (n_col, n_col), 0) == lax.broadcasted_iota(jnp.int32, (n_col, n_col), 1),
-        jnp.ones((n_col, n_col), F32),
-        jnp.zeros((n_col, n_col), F32),
-    ).astype(BF16)
-    turned = lax.dot_general(eye, w_ref[...], (((1,), (1,)), ((), ())), preferred_element_type=F32)
-    wt_s[z, y] = turned.astype(BF16).reshape(2, quarter, width)
-
     load_g.wait()
     load_v.wait()
     sig = jax.nn.sigmoid(g_s[...].astype(F32))
@@ -152,6 +150,8 @@
     halo_send[1] = mixed[:EDGE]
     mpad[EDGE : EDGE + rows] = mixed.astype(F32)
 
+    for load in (load_w, load_taps, load_gain, load_bias):
+        load.wait()
     pl.semaphore_wait(barrier, len(peers))
 
     halo = [
@@ -184,29 +184,31 @@
             for sign in (1, -1):
                 if ring_depth(h, 0, sign) >= 1:
                     forward(h, 0, sign, 1)
+        todo = [(near(d, size(h, 1)), d, h) for h in range(2) for d in range(1, size(h, 1))]
+        for _, d, h in sorted(todo):
+            block = wt_s.at[(*cell(h, place(h, 1), place(h, 2)), h)]
+            first[h, d] = send(block, block, a1_ss.at[h, d], a1_rs.at[h, d], along(h, 1, d))
+
+    def gather_round(r):
+        todo = []
         for h in range(2):
             n = size(h, 1)
-            block = wt_s.at[(*cell(h, place(h, 1), place(h, 2)), h)]
-            for d in sorted(range(1, n), key=lambda d: near(d, n)):
-                first[h, d] = send(block, block, a1_ss.at[h, d], a1_rs.at[h, d], along(h, 1, d))
-
-    def gather_round(r):
-        for h in range(2):
-            n = size(h, 1)
-            for d in sorted(range(n), key=lambda d: near(d, n)):
-                k = r - near(d, n) + 1
+            for d in range(n):
+                k = r - min(near(d, n), 2) + 1
                 if (d == 0 and k == 1) or k < 1 or k > size(h, 2) // 2 + 1:
                     continue
-                if k == 1:
-                    first[h, d].wait_recv()
-                for sign in (1, -1):
-                    depth = ring_depth(h, d, sign)
-                    if 1 <= k - 1 <= depth:
-                        ring[h, d, sign, k - 1].wait_recv()
-                    if k <= depth:
-                        forward(h, d, sign, k)
-
-    rounds = max(size(h, 1) // 2 + size(h, 2) // 2 + 1 for h in range(2))
+                todo.append((near(d, n), d, h, k))
+        for _, d, h, k in sorted(todo):
+            if k == 1:
+                first[h, d].wait_recv()
+            for sign in (1, -1):
+                depth = ring_depth(h, d, sign)
+                if 1 <= k - 1 <= depth:
+                    ring[h, d, sign, k - 1].wait_recv()
+                if k <= depth:
+                    forward(h, d, sign, k)
+
+    rounds = max(min(size(h, 1) // 2, 2) + size(h, 2) // 2 + 1 for h in range(2))
     gather_start()
 
     halo[0].wait_recv()
@@ -230,7 +232,10 @@
         s2_s[pl.ds(base, chunk), :] = fold(total * total)
         return carry
 
-    for i in range(steps):
+    for i in range(2 * steps // 5):
+        conv_step(i, 0)
+    gather_round(1)
+    for i in range(2 * steps // 5, steps):
         conv_step(i, 0)
 
     def row_sums(which):
@@ -262,8 +267,7 @@
         return jnp.transpose(jnp.broadcast_to(row, (lanes, padded_rows)))
 
     sums = row_sums(0)
-    gather_round(0)
-    gather_round(1)
+    gather_round(2)
     total = gathered_sums(0, sums)
     mean = total[0:1]
     inv = lax.rsqrt(total[1:2] - mean * mean + EPS)
@@ -281,7 +285,7 @@
     lax.fori_loop(0, steps, act_step, 0)
     act_s[...] = act_f[...].astype(BF16)
     load_og.wait()
-    gather_round(2)
+    gather_round(3)
 
     block_cols = ny * n_col
 
@@ -293,25 +297,35 @@
         wgt_s[i] = part.reshape(ny, 2, quarter, width)
         return carry
 
-    lax.fori_loop(0, nz, grad_step, 0)
+    lax.fori_loop(0, nz // 2, grad_step, 0)
+    gather_round(4)
+    lax.fori_loop(nz // 2, nz, grad_step, 0)
 
     hops, last = {}, {}
 
+    def parts(h):
+        return min(4, size(h, 1))
+
+    def span_of(h, c):
+        n = size(h, 1) // parts(h)
+        return slice(c * n, (c + 1) * n)
+
     def piece(h, c, p):
-        n = size(h, 1) // 2
         if h == 0:
-            return wgt_s[p, c * n : (c + 1) * n, 0]
-        return wgt_s[c * n : (c + 1) * n, p, 1]
+            return wgt_s[p, span_of(h, c), 0]
+        return wgt_s[span_of(h, c), p, 1]
 
     def reduce_depth(h, c, sign):
         n = size(h, 2)
-        return n // 2 if (c == 0) == (sign > 0) else n // 2 - 1
+        return n // 2 if (c % 2 == 0) == (sign > 0) else n // 2 - 1
 
     def reduce_round(j):
-        for h in range(2):
-            n = size(h, 2)
-            part = pl.ds(0, size(h, 1) // 2)
-            for c in range(2):
+        for c in range(4):
+            for h in range(2):
+                if c >= parts(h):
+                    continue
+                n = size(h, 2)
+                part = pl.ds(0, size(h, 1) // parts(h))
                 for i, sign in enumerate((1, -1)):
                     depth = reduce_depth(h, c, sign)
                     k = j - (n // 2 - depth)
@@ -332,26 +346,28 @@
                     )
 
     def reduce_finish():
-        for h in range(2):
-            n = size(h, 1) // 2
-            for c in range(2):
+        for c in range(4):
+            for h in range(2):
+                if c >= parts(h):
+                    continue
                 value = piece(h, c, place(h, 2))
+                part = pl.ds(0, size(h, 1) // parts(h))
                 for i, sign in enumerate((1, -1)):
                     depth = reduce_depth(h, c, sign)
                     if depth:
                         hops[h, c, sign, depth].wait_recv()
-                        value = value + rs_r[h, c, i, depth - 1, pl.ds(0, n)].astype(F32)
+                        value = value + rs_r[h, c, i, depth - 1, part].astype(F32)
                 if h == 0:
-                    wgt_s[place(h, 2), c * n : (c + 1) * n, 0] = value
+                    wgt_s[place(h, 2), span_of(h, c), 0] = value
                 else:
-                    wgt_s[c * n : (c + 1) * n, place(h, 2), 1] = value
-                q_s[h, c * n : (c + 1) * n] = value.astype(BF16)
-            n = size(h, 1)
-            for d in sorted(range(1, n), key=lambda d: near(d, n)):
-                to = lax.rem(place(h, 1) + d, n)
-                last[h, d] = send(
-                    q_s.at[h, to], q_r.at[h, d], r2_ss.at[h, d], r2_rs.at[h, d], along(h, 1, d)
-                )
+                    wgt_s[span_of(h, c), place(h, 2), 1] = value
+                q_s[h, span_of(h, c)] = value.astype(BF16)
+        todo = [(near(d, size(h, 1)), d, h) for h in range(2) for d in range(1, size(h, 1))]
+        for _, d, h in sorted(todo):
+            to = lax.rem(place(h, 1) + d, size(h, 1))
+            last[h, d] = send(
+                q_s.at[h, to], q_r.at[h, d], r2_ss.at[h, d], r2_rs.at[h, d], along(h, 1, d)
+            )
 
     def reduce_end():
         for h in range(2):
@@ -361,10 +377,10 @@
                 value = value + q_r[h, d].astype(F32)
             wg_ref[h] = value
 
-    gather_round(3)
+    for r in range(5, rounds - 1):
+        gather_round(r)
     reduce_round(1)
-    for r in range(4, rounds):
-        gather_round(r)
+    gather_round(rounds - 1)
     reduce_round(2)
 
     def product_step(i, carry):
@@ -377,7 +393,6 @@
 
     ag_s[...] = jnp.zeros_like(ag_s)
     lax.fori_loop(0, nz, product_step, 0)
-    reduce_round(3)
 
     def pre_step(i, carry):
         gain_sum, bias_sum = carry
@@ -399,7 +414,7 @@
     gain_row = jnp.sum(gain_sum, axis=0, keepdims=True)
     bias_row = jnp.sum(bias_sum, axis=0, keepdims=True)
     sums = row_sums(1)
-    reduce_round(4)
+    reduce_round(3)
     total = gathered_sums(1, sums)
     b1_s[...] = down_rows(total[0:1])
     b2_s[...] = down_rows(total[1:2])
@@ -462,7 +477,7 @@
             small_ref[:, h * lanes : (h + 1) * lanes] = value
 
     small_1 = small_send(1)
-    reduce_finish()
+    reduce_round(4)
 
     back[0].wait_recv()
     back[1].wait_recv()
@@ -481,6 +496,7 @@
         mixed_step(i, 0)
     small_add(1, small_1)
     small_2 = small_send(2)
+    reduce_finish()
     scaled = ag_s[...] * sig_s[...]
     vg_ref[...] = scaled.astype(BF16)
     gg_ref[...] = (scaled * vf_s[...] * (1.0 - sig_s[...])).astype(BF16)
@@ -488,6 +504,15 @@
     small_add(2, small_2)
     for copy in pending:
         copy.wait_send()
+
+
+def finish(span, vg_ref, gg_ref, small_ref, wg_ref, vg_out, gg_out, tap_out, gain_out, bias_out, wg_out):
+    vg_out[...] = vg_ref[...]
+    gg_out[...] = gg_ref[...]
+    wg_out[...] = wg_ref[...]
+    tap_out[...] = small_ref[:span]
+    gain_out[...] = small_ref[span : span + 1]
+    bias_out[...] = small_ref[span + 1 : span + 2]
 
 
 def on_device(sizes, value_in, gate_in, taps, norm_gain, norm_bias, proj_weight, out_grad):
@@ -505,7 +530,7 @@
     n_half = n_max // 2
     dma = pltpu.SemaphoreType.DMA
     vmem = pl.BlockSpec(memory_space=pltpu.VMEM)
-    anywhere = pl.BlockSpec(memory_space=pl.ANY)
+    hbm = pl.BlockSpec(memory_space=pltpu.HBM)
     cfg = (nz, ny, nt, rows, width, span, chunk)
     vg, gg, small, wg = pl.pallas_call(
         functools.partial(kernel, cfg),
@@ -515,12 +540,15 @@
             jax.ShapeDtypeStruct((small_rows, width), F32),
             jax.ShapeDtypeStruct((2, quarter, width), F32),
         ),
-        in_specs=[anywhere, anywhere, vmem, vmem, vmem, vmem, anywhere],
+        in_specs=[hbm] * 7,
         out_specs=(vmem, vmem, vmem, vmem),
         scratch_shapes=[
             pltpu.VMEM((rows, width), BF16),
             pltpu.VMEM((rows, width), BF16),
             pltpu.VMEM((rows, columns), BF16),
+            pltpu.VMEM((span, width), F32),
+            pltpu.VMEM((1, width), F32),
+            pltpu.VMEM((1, width), F32),
             pltpu.VMEM((rows, width), F32),
             pltpu.VMEM((rows, width), F32),
             pltpu.VMEM((rows + 2 * EDGE, width), F32),
@@ -542,13 +570,13 @@
             pltpu.VMEM((2, nt, 2, padded_rows), F32),
             pltpu.VMEM((nz, ny, 2, quarter, width), BF16),
             pltpu.VMEM((nz, ny, 2, quarter, width), F32),
-            pltpu.VMEM((2, 2, 2, n_half, n_half, quarter, width), BF16),
-            pltpu.VMEM((2, 2, 2, n_half, n_half, quarter, width), BF16),
+            pltpu.VMEM((2, 4, 2, n_half, max(1, n_max // 4), quarter, width), BF16),
+            pltpu.VMEM((2, 4, 2, n_half, max(1, n_max // 4), quarter, width), BF16),
             pltpu.VMEM((2, n_max, quarter, width), BF16),
             pltpu.VMEM((2, n_max, quarter, width), BF16),
             pltpu.VMEM((2, 2, small_rows, lanes), BF16),
             pltpu.VMEM((2, 2, n_max, small_rows, lanes), BF16),
-            dma((3,)),
+            dma((7,)),
             dma((4,)),
             dma((4,)),
             dma((2, nt)),
@@ -557,8 +585,8 @@
             dma((2, n_max)),
             dma((2, n_max, 2, n_half)),
             dma((2, n_max, 2, n_half)),
-            dma((2, 2, 2, n_half)),
-            dma((2, 2, 2, n_half)),
+            dma((2, 4, 2, n_half)),
+            dma((2, 4, 2, n_half)),
             dma((2, n_max)),
             dma((2, n_max)),
             dma((2, 2, n_max)),
@@ -568,9 +596,31 @@
             collective_id=0, has_side_effects=True, vmem_limit_bytes=60 * 1024 * 1024
         ),
         name="step",
-    )(value_in, gate_in, taps, norm_gain[None, :], norm_bias[None, :], proj_weight, out_grad)
-    weight_grad = jnp.transpose(wg.reshape(n_col, width))
-    return (vg, gg, small[:span], small[span], small[span + 1], weight_grad)
+    )(
+        value_in,
+        gate_in,
+        taps,
+        norm_gain[None, :],
+        norm_bias[None, :],
+        proj_weight.T.reshape(2, quarter, width),
+        out_grad,
+    )
+    vg, gg, tap, gain, bias, wg = pl.pallas_call(
+        functools.partial(finish, span),
+        out_shape=(
+            jax.ShapeDtypeStruct((rows, width), BF16),
+            jax.ShapeDtypeStruct((rows, width), BF16),
+            jax.ShapeDtypeStruct((span, width), F32),
+            jax.ShapeDtypeStruct((1, width), F32),
+            jax.ShapeDtypeStruct((1, width), F32),
+            jax.ShapeDtypeStruct((2, quarter, width), F32),
+        ),
+        in_specs=[vmem] * 4,
+        out_specs=(vmem,) * 6,
+        compiler_params=pltpu.CompilerParams(vmem_limit_bytes=60 * 1024 * 1024),
+        name="finish",
+    )(vg, gg, small, wg)
+    return (vg, gg, tap, gain[0], bias[0], jnp.transpose(wg.reshape(n_col, width)))
 
 
 def solution(mesh):

time: 86.9 us -> 69.7 us (0.80)
  the two profiles are of different devices: /device:TPU:8 before, /device:TPU:1 now
where the time goes in v2:
time: 69.7 us; the launch traced here: 69.5 us
  Pallas kernels  68.9 us (99%)
    pallas_call x1, Pallas kernels, on_device(): pl.pallas_call(functools.partial(kernel, cfg), out_shape=(jax.ShapeDtypeS...  67.1 us
    pallas_call x1, Pallas kernels, on_device(): pl.pallas_call(functools.partial(finish, span), out_shape=(jax.ShapeDtype...  1.82 us

profile of v2, /device:TPU:1, one launch (start us, length us, event | category | flops | bytes accessed | tf_op | source)
XLA Modules:
  0.0 69.5 jit_solution(18038279801423971744)
XLA Ops:
  0.6 67.1 %step.1 = (bf16[360,256]{1,0:T(8,128)(2,1)}, bf16[360,256]{1,0:T(8,128)(2,1)}, f32[48,256]{1,0:T(8,128)}, f32[2,32,256]{2,1,0:T(8,128)}) custom-call(bf16[360,256]{1,0:T(8,128)(2,1)} %v_hbm.1, bf16[360,256]{1,0:T(8,128)(2,1)} %g_hbm.1, f32[31,256]{1,0:T(8,128)} %taps_hbm.1, f32[1,256]{1,0:T(1,128)} %bitcast.11, f32[1,256]{1,0:T(1,128)} %bitcast.12, ...), custom_call_target="tpu_custom_call" | custom-call | tf_op jit(solution)/shard_map/step/pallas_call | solution.py:535
  67.7 1.8 %finish.1 = (bf16[360,256]{1,0:T(8,128)(2,1)}, bf16[360,256]{1,0:T(8,128)(2,1)}, f32[31,256]{1,0:T(8,128)}, f32[1,256]{1,0:T(1,128)}, f32[1,256]{1,0:T(1,128)}, /*index=5*/f32[2,32,256]{2,1,0:T(8,128)}) custom-call(bf16[360,256]{1,0:T(8,128)(2,1)} %get-tuple-element.16.vg_ref, bf16[360,256]{1,0:T(8,128)(2,1)} %get-tuple-element.17.gg_ref, ...), custom_call_target="tpu_custom_call" | custom-call | tf_op jit(solution)/shard_map/finish/pallas_call | solution.py:608

commit v3 on v2

--- a/solution.py
+++ b/solution.py
@@ -25,8 +25,8 @@
     bias_hbm,
     w_hbm,
     og_hbm,
-    vg_ref,
-    gg_ref,
+    vg_hbm,
+    gg_hbm,
     small_ref,
     wg_ref,
     v_s,
@@ -189,13 +189,13 @@
             block = wt_s.at[(*cell(h, place(h, 1), place(h, 2)), h)]
             first[h, d] = send(block, block, a1_ss.at[h, d], a1_rs.at[h, d], along(h, 1, d))
 
-    def gather_round(r):
+    def gather_round(r, low=0, high=99):
         todo = []
         for h in range(2):
             n = size(h, 1)
             for d in range(n):
-                k = r - min(near(d, n), 2) + 1
-                if (d == 0 and k == 1) or k < 1 or k > size(h, 2) // 2 + 1:
+                k = r - min(near(d, n), 1) + 1
+                if (d == 0 and k == 1) or k < 1 or k > size(h, 2) // 2 + 1 or not low <= near(d, n) <= high:
                     continue
                 todo.append((near(d, n), d, h, k))
         for _, d, h, k in sorted(todo):
@@ -208,11 +208,13 @@
                 if k <= depth:
                     forward(h, d, sign, k)
 
-    rounds = max(min(size(h, 1) // 2, 2) + size(h, 2) // 2 + 1 for h in range(2))
+    rounds = max(size(h, 2) // 2 + 2 for h in range(2))
     gather_start()
+    gather_round(1, 0, 2)
 
     halo[0].wait_recv()
     halo[1].wait_recv()
+    gather_round(1, 3)
     mpad[:EDGE] = jnp.where(s == 0, 0.0, halo_recv[0].astype(F32))
     mpad[EDGE + rows :] = jnp.where(s == count - 1, 0.0, halo_recv[1].astype(F32))
 
@@ -232,10 +234,7 @@
         s2_s[pl.ds(base, chunk), :] = fold(total * total)
         return carry
 
-    for i in range(2 * steps // 5):
-        conv_step(i, 0)
-    gather_round(1)
-    for i in range(2 * steps // 5, steps):
+    for i in range(steps):
         conv_step(i, 0)
 
     def row_sums(which):
@@ -268,6 +267,7 @@
 
     sums = row_sums(0)
     gather_round(2)
+    gather_round(3)
     total = gathered_sums(0, sums)
     mean = total[0:1]
     inv = lax.rsqrt(total[1:2] - mean * mean + EPS)
@@ -285,7 +285,6 @@
     lax.fori_loop(0, steps, act_step, 0)
     act_s[...] = act_f[...].astype(BF16)
     load_og.wait()
-    gather_round(3)
 
     block_cols = ny * n_col
 
@@ -362,7 +361,7 @@
                 else:
                     wgt_s[span_of(h, c), place(h, 2), 1] = value
                 q_s[h, span_of(h, c)] = value.astype(BF16)
-        todo = [(near(d, size(h, 1)), d, h) for h in range(2) for d in range(1, size(h, 1))]
+        todo = [(-near(d, size(h, 1)), d, h) for h in range(2) for d in range(1, size(h, 1))]
         for _, d, h in sorted(todo):
             to = lax.rem(place(h, 1) + d, size(h, 1))
             last[h, d] = send(
@@ -381,7 +380,6 @@
         gather_round(r)
     reduce_round(1)
     gather_round(rounds - 1)
-    reduce_round(2)
 
     def product_step(i, carry):
         columns = pl.ds(pl.multiple_of(i * block_cols, 128), block_cols)
@@ -393,6 +391,7 @@
 
     ag_s[...] = jnp.zeros_like(ag_s)
     lax.fori_loop(0, nz, product_step, 0)
+    reduce_round(2)
 
     def pre_step(i, carry):
         gain_sum, bias_sum = carry
@@ -456,16 +455,15 @@
         copies = {}
         for h in range(2):
             ar_s[phase - 1, h] = small_ref[:, h * lanes : (h + 1) * lanes].astype(BF16)
-        for h in range(2):
-            n = size(h, phase)
-            for d in sorted(range(1, n), key=lambda d: near(d, n)):
-                copies[h, d] = send(
-                    ar_s.at[phase - 1, h],
-                    ar_r.at[phase - 1, h, d],
-                    ar_ss.at[phase - 1, h, d],
-                    ar_rs.at[phase - 1, h, d],
-                    along(h, phase, d),
-                )
+        todo = [(-near(d, size(h, phase)), d, h) for h in range(2) for d in range(1, size(h, phase))]
+        for _, d, h in sorted(todo):
+            copies[h, d] = send(
+                ar_s.at[phase - 1, h],
+                ar_r.at[phase - 1, h, d],
+                ar_ss.at[phase - 1, h, d],
+                ar_rs.at[phase - 1, h, d],
+                along(h, phase, d),
+            )
         return copies
 
     def small_add(phase, copies):
@@ -494,14 +492,20 @@
 
     for i in range(steps):
         mixed_step(i, 0)
+    reduce_finish()
     small_add(1, small_1)
     small_2 = small_send(2)
-    reduce_finish()
     scaled = ag_s[...] * sig_s[...]
-    vg_ref[...] = scaled.astype(BF16)
-    gg_ref[...] = (scaled * vf_s[...] * (1.0 - sig_s[...])).astype(BF16)
+    v_s[...] = scaled.astype(BF16)
+    g_s[...] = (scaled * vf_s[...] * (1.0 - sig_s[...])).astype(BF16)
+    store_v = pltpu.make_async_copy(v_s, vg_hbm, local_sem.at[0])
+    store_g = pltpu.make_async_copy(g_s, gg_hbm, local_sem.at[1])
+    store_v.start()
+    store_g.start()
     reduce_end()
     small_add(2, small_2)
+    store_v.wait()
+    store_g.wait()
     for copy in pending:
         copy.wait_send()
 
@@ -525,7 +529,7 @@
     lanes = width // 2
     chunk = next(c for c in (72, 24, 8) if rows % c == 0)
     padded_rows = (rows + 127) // 128 * 128
-    small_rows = (span + 2 + 15) // 16 * 16
+    small_rows = (span + 2 + 7) // 8 * 8
     n_max = max(nz, ny)
     n_half = n_max // 2
     dma = pltpu.SemaphoreType.DMA
@@ -541,7 +545,7 @@
             jax.ShapeDtypeStruct((2, quarter, width), F32),
         ),
         in_specs=[hbm] * 7,
-        out_specs=(vmem, vmem, vmem, vmem),
+        out_specs=(hbm, hbm, vmem, vmem),
         scratch_shapes=[
             pltpu.VMEM((rows, width), BF16),
             pltpu.VMEM((rows, width), BF16),

time: 69.7 us -> 68 us (0.976)
  Pallas kernels: 68.9 us -> 67.2 us
    pallas_call x1, Pallas kernels: 67.1 us -> 65.4 us  [on_device(): pl.pallas_call(functools.partial(kernel, cfg), out_shape=(jax.ShapeDtypeS...]
where the time goes in v3:
time: 68 us; the launch traced here: 67.9 us
  Pallas kernels  67.2 us (99%)
    pallas_call x1, Pallas kernels, on_device(): pl.pallas_call(functools.partial(kernel, cfg), out_shape=(jax.ShapeDtypeS...  65.4 us
    pallas_call x1, Pallas kernels, on_device(): pl.pallas_call(functools.partial(finish, span), out_shape=(jax.ShapeDtype...  1.82 us

profile of v3, /device:TPU:1, one launch (start us, length us, event | category | flops | bytes accessed | tf_op | source)
XLA Modules:
  0.0 67.9 jit_solution(225510267674144775)
XLA Ops:
  0.6 65.4 %step.1 = (bf16[360,256]{1,0:T(8,128)(2,1)}, bf16[360,256]{1,0:T(8,128)(2,1)}, f32[40,256]{1,0:T(8,128)}, f32[2,32,256]{2,1,0:T(8,128)}) custom-call(bf16[360,256]{1,0:T(8,128)(2,1)} %v_hbm.1, bf16[360,256]{1,0:T(8,128)(2,1)} %g_hbm.1, f32[31,256]{1,0:T(8,128)} %taps_hbm.1, f32[1,256]{1,0:T(1,128)} %bitcast.11, f32[1,256]{1,0:T(1,128)} %bitcast.12, ...), custom_call_target="tpu_custom_call" | custom-call | tf_op jit(solution)/shard_map/step/pallas_call | solution.py:539
  66.1 1.8 %finish.1 = (bf16[360,256]{1,0:T(8,128)(2,1)}, bf16[360,256]{1,0:T(8,128)(2,1)}, f32[31,256]{1,0:T(8,128)}, f32[1,256]{1,0:T(1,128)}, f32[1,256]{1,0:T(1,128)}, /*index=5*/f32[2,32,256]{2,1,0:T(8,128)}) custom-call(bf16[360,256]{1,0:T(8,128)(2,1)} %get-tuple-element.16.vg_ref, bf16[360,256]{1,0:T(8,128)(2,1)} %get-tuple-element.17.gg_ref, ...), custom_call_target="tpu_custom_call" | custom-call | tf_op jit(solution)/shard_map/finish/pallas_call | solution.py:612

commit v4 on v3

--- a/solution.py
+++ b/solution.py
@@ -63,19 +63,12 @@
     ar_s,
     ar_r,
     local_sem,
-    halo_ss,
+    send_sem,
     halo_rs,
-    st_ss,
     st_rs,
-    a1_ss,
     a1_rs,
-    a2_ss,
     a2_rs,
-    r1_ss,
-    r1_rs,
-    r2_ss,
     r2_rs,
-    ar_ss,
     ar_rs,
 ):
     nz, ny, nt, rows, width, span, chunk = cfg
@@ -108,10 +101,19 @@
         return (b, a) if h == 0 else (a, b)
 
     pending = []
-
-    def send(src, dst, ssem, rsem, dev):
+    slots = send_sem.shape[0]
+
+    def send(src, dst, rsem, dev):
+        slot = len(pending) % slots
+        if len(pending) >= slots:
+            pending[-slots].wait_send()
         copy = pltpu.make_async_remote_copy(
-            src_ref=src, dst_ref=dst, send_sem=ssem, recv_sem=rsem, device_id=dev, device_id_type=MESH
+            src_ref=src,
+            dst_ref=dst,
+            send_sem=send_sem.at[slot],
+            recv_sem=rsem,
+            device_id=dev,
+            device_id_type=MESH,
         )
         copy.start()
         pending.append(copy)
@@ -155,8 +157,8 @@
     pl.semaphore_wait(barrier, len(peers))
 
     halo = [
-        send(halo_send.at[0], halo_recv.at[0], halo_ss.at[0], halo_rs.at[0], right_dev),
-        send(halo_send.at[1], halo_recv.at[1], halo_ss.at[1], halo_rs.at[1], left_dev),
+        send(halo_send.at[0], halo_recv.at[0], halo_rs.at[0], right_dev),
+        send(halo_send.at[1], halo_recv.at[1], halo_rs.at[1], left_dev),
     ]
 
     first, ring = {}, {}
@@ -176,7 +178,7 @@
         block = wt_s.at[(*cell(h, a, b), h)]
         i = 0 if sign > 0 else 1
         ring[h, d, sign, k] = send(
-            block, block, a2_ss.at[h, d, i, k - 1], a2_rs.at[h, d, i, k - 1], along(h, 2, sign)
+            block, block, a2_rs.at[h, d, i, k - 1], along(h, 2, sign)
         )
 
     def gather_start():
@@ -187,7 +189,7 @@
         todo = [(near(d, size(h, 1)), d, h) for h in range(2) for d in range(1, size(h, 1))]
         for _, d, h in sorted(todo):
             block = wt_s.at[(*cell(h, place(h, 1), place(h, 2)), h)]
-            first[h, d] = send(block, block, a1_ss.at[h, d], a1_rs.at[h, d], along(h, 1, d))
+            first[h, d] = send(block, block, a1_rs.at[h, d], along(h, 1, d))
 
     def gather_round(r, low=0, high=99):
         todo = []
@@ -248,7 +250,6 @@
                 send(
                     st_send.at[which],
                     st_recv.at[which, d],
-                    st_ss.at[which, d],
                     st_rs.at[which, d],
                     at(z, y, lax.rem(t + d, nt)),
                 )
@@ -305,14 +306,14 @@
     def parts(h):
         return min(4, size(h, 1))
 
-    def span_of(h, c):
-        n = size(h, 1) // parts(h)
-        return slice(c * n, (c + 1) * n)
-
-    def piece(h, c, p):
-        if h == 0:
-            return wgt_s[p, span_of(h, c), 0]
-        return wgt_s[span_of(h, c), p, 1]
+    def shifts(h, c):
+        n = size(h, 1)
+        order = sorted(range(n), key=lambda d: (-near(d, n), d))
+        return order[c * n // parts(h) : (c + 1) * n // parts(h)]
+
+    def term(h, shift, dest):
+        q = lax.rem(place(h, 1) + shift, size(h, 1))
+        return wgt_s[(*cell(h, q, dest), h)]
 
     def reduce_depth(h, c, sign):
         n = size(h, 2)
@@ -331,16 +332,17 @@
                     if k < 1 or k > depth:
                         continue
                     dest = lax.rem(place(h, 2) + sign * (depth - k + 1) + n, n)
-                    value = piece(h, c, dest)
                     if k > 1:
                         hops[h, c, sign, k - 1].wait_recv()
-                        value = value + rs_r[h, c, i, k - 2, part].astype(F32)
-                    rs_s[h, c, i, k - 1, part] = value.astype(BF16)
+                    for j_at, shift in enumerate(shifts(h, c)):
+                        value = term(h, shift, dest)
+                        if k > 1:
+                            value = value + rs_r[h, c, i, k - 2, j_at].astype(F32)
+                        rs_s[h, c, i, k - 1, j_at] = value.astype(BF16)
                     hops[h, c, sign, k] = send(
                         rs_s.at[h, c, i, k - 1, part],
                         rs_r.at[h, c, i, k - 1, part],
-                        r1_ss.at[h, c, i, k - 1],
-                        r1_rs.at[h, c, i, k - 1],
+                        a2_rs.at[h, 2 * c + (k - 1) // 2, i, (k - 1) % 2],
                         along(h, 2, sign),
                     )
 
@@ -349,24 +351,21 @@
             for h in range(2):
                 if c >= parts(h):
                     continue
-                value = piece(h, c, place(h, 2))
-                part = pl.ds(0, size(h, 1) // parts(h))
                 for i, sign in enumerate((1, -1)):
-                    depth = reduce_depth(h, c, sign)
-                    if depth:
-                        hops[h, c, sign, depth].wait_recv()
-                        value = value + rs_r[h, c, i, depth - 1, part].astype(F32)
-                if h == 0:
-                    wgt_s[place(h, 2), span_of(h, c), 0] = value
-                else:
-                    wgt_s[span_of(h, c), place(h, 2), 1] = value
-                q_s[h, span_of(h, c)] = value.astype(BF16)
-        todo = [(-near(d, size(h, 1)), d, h) for h in range(2) for d in range(1, size(h, 1))]
-        for _, d, h in sorted(todo):
-            to = lax.rem(place(h, 1) + d, size(h, 1))
-            last[h, d] = send(
-                q_s.at[h, to], q_r.at[h, d], r2_ss.at[h, d], r2_rs.at[h, d], along(h, 1, d)
-            )
+                    if reduce_depth(h, c, sign):
+                        hops[h, c, sign, reduce_depth(h, c, sign)].wait_recv()
+                for j_at, shift in enumerate(shifts(h, c)):
+                    value = term(h, shift, place(h, 2))
+                    for i, sign in enumerate((1, -1)):
+                        if reduce_depth(h, c, sign):
+                            value = value + rs_r[h, c, i, reduce_depth(h, c, sign) - 1, j_at].astype(F32)
+                    if shift == 0:
+                        wgt_s[z, y, h] = value
+                        continue
+                    q_s[h, shift] = value.astype(BF16)
+                    last[h, shift] = send(
+                        q_s.at[h, shift], q_r.at[h, shift], r2_rs.at[h, shift], along(h, 1, shift)
+                    )
 
     def reduce_end():
         for h in range(2):
@@ -429,8 +428,8 @@
 
     lax.fori_loop(0, steps, conv_grad_step, 0)
     back = [
-        send(cgpad.at[pl.ds(rows, EDGE)], cg_recv.at[0], halo_ss.at[2], halo_rs.at[2], right_dev),
-        send(cgpad.at[pl.ds(EDGE, EDGE)], cg_recv.at[1], halo_ss.at[3], halo_rs.at[3], left_dev),
+        send(cgpad.at[pl.ds(rows, EDGE)], cg_recv.at[0], halo_rs.at[2], right_dev),
+        send(cgpad.at[pl.ds(EDGE, EDGE)], cg_recv.at[1], halo_rs.at[3], left_dev),
     ]
 
     tacc[...] = jnp.zeros_like(tacc)
@@ -460,7 +459,6 @@
             copies[h, d] = send(
                 ar_s.at[phase - 1, h],
                 ar_r.at[phase - 1, h, d],
-                ar_ss.at[phase - 1, h, d],
                 ar_rs.at[phase - 1, h, d],
                 along(h, phase, d),
             )
@@ -506,7 +504,7 @@
     small_add(2, small_2)
     store_v.wait()
     store_g.wait()
-    for copy in pending:
+    for copy in pending[-slots:]:
         copy.wait_send()
 
 
@@ -581,19 +579,12 @@
             pltpu.VMEM((2, 2, small_rows, lanes), BF16),
             pltpu.VMEM((2, 2, n_max, small_rows, lanes), BF16),
             dma((7,)),
-            dma((4,)),
+            dma((40,)),
             dma((4,)),
             dma((2, nt)),
-            dma((2, nt)),
-            dma((2, n_max)),
             dma((2, n_max)),
             dma((2, n_max, 2, n_half)),
-            dma((2, n_max, 2, n_half)),
-            dma((2, 4, 2, n_half)),
-            dma((2, 4, 2, n_half)),
             dma((2, n_max)),
-            dma((2, n_max)),
-            dma((2, 2, n_max)),
             dma((2, 2, n_max)),
         ],
         compiler_params=pltpu.CompilerParams(

time: 68 us -> 62.7 us (0.922)
  Pallas kernels: 67.2 us -> 61.8 us
    pallas_call x1, Pallas kernels: 65.4 us -> 60 us  [on_device(): pl.pallas_call(functools.partial(kernel, cfg), out_shape=(jax.ShapeDtypeS...]
where the time goes in v4:
time: 62.7 us; the launch traced here: 62.4 us
  Pallas kernels  61.8 us (99%)
  between operations  0.64 us (1%)
    pallas_call x1, Pallas kernels, on_device(): pl.pallas_call(functools.partial(kernel, cfg), out_shape=(jax.ShapeDtypeS...  60 us
    pallas_call x1, Pallas kernels, on_device(): pl.pallas_call(functools.partial(finish, span), out_shape=(jax.ShapeDtype...  1.82 us

profile of v4, /device:TPU:1, one launch (start us, length us, event | category | flops | bytes accessed | tf_op | source)
XLA Modules:
  0.0 62.4 jit_solution(17091940101724917627)
XLA Ops:
  0.6 60.0 %step.1 = (bf16[360,256]{1,0:T(8,128)(2,1)}, bf16[360,256]{1,0:T(8,128)(2,1)}, f32[40,256]{1,0:T(8,128)}, f32[2,32,256]{2,1,0:T(8,128)}) custom-call(bf16[360,256]{1,0:T(8,128)(2,1)} %v_hbm.1, bf16[360,256]{1,0:T(8,128)(2,1)} %g_hbm.1, f32[31,256]{1,0:T(8,128)} %taps_hbm.1, f32[1,256]{1,0:T(1,128)} %bitcast.11, f32[1,256]{1,0:T(1,128)} %bitcast.12, ...), custom_call_target="tpu_custom_call" | custom-call | tf_op jit(solution)/shard_map/step/pallas_call | solution.py:537
  60.6 1.8 %finish.1 = (bf16[360,256]{1,0:T(8,128)(2,1)}, bf16[360,256]{1,0:T(8,128)(2,1)}, f32[31,256]{1,0:T(8,128)}, f32[1,256]{1,0:T(1,128)}, f32[1,256]{1,0:T(1,128)}, /*index=5*/f32[2,32,256]{2,1,0:T(8,128)}) custom-call(bf16[360,256]{1,0:T(8,128)(2,1)} %get-tuple-element.16.vg_ref, bf16[360,256]{1,0:T(8,128)(2,1)} %get-tuple-element.17.gg_ref, ...), custom_call_target="tpu_custom_call" | custom-call | tf_op jit(solution)/shard_map/finish/pallas_call | solution.py:603

commit v5 on v4

--- a/solution.py
+++ b/solution.py
@@ -178,7 +178,7 @@
         block = wt_s.at[(*cell(h, a, b), h)]
         i = 0 if sign > 0 else 1
         ring[h, d, sign, k] = send(
-            block, block, a2_rs.at[h, d, i, k - 1], along(h, 2, sign)
+            block, block, a2_rs.at[h, d, i * (n // 2 - 1) + k - 1 if k < n // 2 else n - 2], along(h, 2, sign)
         )
 
     def gather_start():
@@ -189,7 +189,7 @@
         todo = [(near(d, size(h, 1)), d, h) for h in range(2) for d in range(1, size(h, 1))]
         for _, d, h in sorted(todo):
             block = wt_s.at[(*cell(h, place(h, 1), place(h, 2)), h)]
-            first[h, d] = send(block, block, a1_rs.at[h, d], along(h, 1, d))
+            first[h, d] = send(block, block, a1_rs.at[h, d - 1], along(h, 1, d))
 
     def gather_round(r, low=0, high=99):
         todo = []
@@ -250,7 +250,7 @@
                 send(
                     st_send.at[which],
                     st_recv.at[which, d],
-                    st_rs.at[which, d],
+                    st_rs.at[which, d - 1],
                     at(z, y, lax.rem(t + d, nt)),
                 )
             )
@@ -342,12 +342,12 @@
                     hops[h, c, sign, k] = send(
                         rs_s.at[h, c, i, k - 1, part],
                         rs_r.at[h, c, i, k - 1, part],
-                        a2_rs.at[h, 2 * c + (k - 1) // 2, i, (k - 1) % 2],
+                        a2_rs.at[h, 2 * c + (k - 1) // 2, i * (n // 2 - 1) + (k - 1) % 2],
                         along(h, 2, sign),
                     )
 
-    def reduce_finish():
-        for c in range(4):
+    def reduce_finish(chunks):
+        for c in chunks:
             for h in range(2):
                 if c >= parts(h):
                     continue
@@ -364,7 +364,7 @@
                         continue
                     q_s[h, shift] = value.astype(BF16)
                     last[h, shift] = send(
-                        q_s.at[h, shift], q_r.at[h, shift], r2_rs.at[h, shift], along(h, 1, shift)
+                        q_s.at[h, shift], q_r.at[h, shift], r2_rs.at[h, shift - 1], along(h, 1, shift)
                     )
 
     def reduce_end():
@@ -389,8 +389,9 @@
         return carry
 
     ag_s[...] = jnp.zeros_like(ag_s)
-    lax.fori_loop(0, nz, product_step, 0)
+    lax.fori_loop(0, nz // 2, product_step, 0)
     reduce_round(2)
+    lax.fori_loop(nz // 2, nz, product_step, 0)
 
     def pre_step(i, carry):
         gain_sum, bias_sum = carry
@@ -459,7 +460,7 @@
             copies[h, d] = send(
                 ar_s.at[phase - 1, h],
                 ar_r.at[phase - 1, h, d],
-                ar_rs.at[phase - 1, h, d],
+                ar_rs.at[phase - 1, h, d - 1],
                 along(h, phase, d),
             )
         return copies
@@ -490,7 +491,7 @@
 
     for i in range(steps):
         mixed_step(i, 0)
-    reduce_finish()
+    reduce_finish(range(4))
     small_add(1, small_1)
     small_2 = small_send(2)
     scaled = ag_s[...] * sig_s[...]
@@ -579,13 +580,13 @@
             pltpu.VMEM((2, 2, small_rows, lanes), BF16),
             pltpu.VMEM((2, 2, n_max, small_rows, lanes), BF16),
             dma((7,)),
-            dma((40,)),
+            dma((32,)),
             dma((4,)),
-            dma((2, nt)),
-            dma((2, n_max)),
-            dma((2, n_max, 2, n_half)),
-            dma((2, n_max)),
-            dma((2, 2, n_max)),
+            dma((2, nt - 1)),
+            dma((2, n_max - 1)),
+            dma((2, n_max, n_max - 1)),
+            dma((2, n_max - 1)),
+            dma((2, 2, n_max - 1)),
         ],
         compiler_params=pltpu.CompilerParams(
             collective_id=0, has_side_effects=True, vmem_limit_bytes=60 * 1024 * 1024

time: 62.7 us -> 63.5 us (1.013)
  Pallas kernels: 61.8 us -> 62.8 us
    pallas_call x1, Pallas kernels: 60 us -> 60.9 us  [on_device(): pl.pallas_call(functools.partial(kernel, cfg), out_shape=(jax.ShapeDtypeS...]
where the time goes in v5:
time: 63.5 us; the launch traced here: 63.4 us
  Pallas kernels  62.8 us (99%)
  between operations  0.64 us (1%)
    pallas_call x1, Pallas kernels, on_device(): pl.pallas_call(functools.partial(kernel, cfg), out_shape=(jax.ShapeDtypeS...  60.9 us
    pallas_call x1, Pallas kernels, on_device(): pl.pallas_call(functools.partial(finish, span), out_shape=(jax.ShapeDtype...  1.82 us

profile of v5, /device:TPU:1, one launch (start us, length us, event | category | flops | bytes accessed | tf_op | source)
XLA Modules:
  0.0 63.4 jit_solution(5800633683817993719)
XLA Ops:
  0.6 60.9 %step.1 = (bf16[360,256]{1,0:T(8,128)(2,1)}, bf16[360,256]{1,0:T(8,128)(2,1)}, f32[40,256]{1,0:T(8,128)}, f32[2,32,256]{2,1,0:T(8,128)}) custom-call(bf16[360,256]{1,0:T(8,128)(2,1)} %v_hbm.1, bf16[360,256]{1,0:T(8,128)(2,1)} %g_hbm.1, f32[31,256]{1,0:T(8,128)} %taps_hbm.1, f32[1,256]{1,0:T(1,128)} %bitcast.11, f32[1,256]{1,0:T(1,128)} %bitcast.12, ...), custom_call_target="tpu_custom_call" | custom-call | tf_op jit(solution)/shard_map/step/pallas_call | solution.py:538
  61.6 1.8 %finish.1 = (bf16[360,256]{1,0:T(8,128)(2,1)}, bf16[360,256]{1,0:T(8,128)(2,1)}, f32[31,256]{1,0:T(8,128)}, f32[1,256]{1,0:T(1,128)}, f32[1,256]{1,0:T(1,128)}, /*index=5*/f32[2,32,256]{2,1,0:T(8,128)}) custom-call(bf16[360,256]{1,0:T(8,128)(2,1)} %get-tuple-element.16.vg_ref, bf16[360,256]{1,0:T(8,128)(2,1)} %get-tuple-element.17.gg_ref, ...), custom_call_target="tpu_custom_call" | custom-call | tf_op jit(solution)/shard_map/finish/pallas_call | solution.py:604

commit v6 on v5

--- a/solution.py
+++ b/solution.py
@@ -389,9 +389,8 @@
         return carry
 
     ag_s[...] = jnp.zeros_like(ag_s)
-    lax.fori_loop(0, nz // 2, product_step, 0)
+    lax.fori_loop(0, nz, product_step, 0)
     reduce_round(2)
-    lax.fori_loop(nz // 2, nz, product_step, 0)
 
     def pre_step(i, carry):
         gain_sum, bias_sum = carry
@@ -491,9 +490,10 @@
 
     for i in range(steps):
         mixed_step(i, 0)
-    reduce_finish(range(4))
+    reduce_finish((0, 1, 2))
     small_add(1, small_1)
     small_2 = small_send(2)
+    reduce_finish((3,))
     scaled = ag_s[...] * sig_s[...]
     v_s[...] = scaled.astype(BF16)
     g_s[...] = (scaled * vf_s[...] * (1.0 - sig_s[...])).astype(BF16)
@@ -580,7 +580,7 @@
             pltpu.VMEM((2, 2, small_rows, lanes), BF16),
             pltpu.VMEM((2, 2, n_max, small_rows, lanes), BF16),
             dma((7,)),
-            dma((32,)),
+            dma((40,)),
             dma((4,)),
             dma((2, nt - 1)),
             dma((2, n_max - 1)),

time: 63.5 us -> 62.5 us (0.984)
  Pallas kernels: 62.8 us -> 61.7 us
    pallas_call x1, Pallas kernels: 60.9 us -> 59.9 us  [on_device(): pl.pallas_call(functools.partial(kernel, cfg), out_shape=(jax.ShapeDtypeS...]
where the time goes in v6:
time: 62.5 us; the launch traced here: 62.3 us
  Pallas kernels  61.7 us (99%)
  between operations  0.64 us (1%)
    pallas_call x1, Pallas kernels, on_device(): pl.pallas_call(functools.partial(kernel, cfg), out_shape=(jax.ShapeDtypeS...  59.9 us
    pallas_call x1, Pallas kernels, on_device(): pl.pallas_call(functools.partial(finish, span), out_shape=(jax.ShapeDtype...  1.82 us

profile of v6, /device:TPU:1, one launch (start us, length us, event | category | flops | bytes accessed | tf_op | source)
XLA Modules:
  0.0 62.3 jit_solution(3869119671624934811)
XLA Ops:
  0.6 59.9 %step.1 = (bf16[360,256]{1,0:T(8,128)(2,1)}, bf16[360,256]{1,0:T(8,128)(2,1)}, f32[40,256]{1,0:T(8,128)}, f32[2,32,256]{2,1,0:T(8,128)}) custom-call(bf16[360,256]{1,0:T(8,128)(2,1)} %v_hbm.1, bf16[360,256]{1,0:T(8,128)(2,1)} %g_hbm.1, f32[31,256]{1,0:T(8,128)} %taps_hbm.1, f32[1,256]{1,0:T(1,128)} %bitcast.11, f32[1,256]{1,0:T(1,128)} %bitcast.12, ...), custom_call_target="tpu_custom_call" | custom-call | tf_op jit(solution)/shard_map/step/pallas_call | solution.py:538
  60.5 1.8 %finish.1 = (bf16[360,256]{1,0:T(8,128)(2,1)}, bf16[360,256]{1,0:T(8,128)(2,1)}, f32[31,256]{1,0:T(8,128)}, f32[1,256]{1,0:T(1,128)}, f32[1,256]{1,0:T(1,128)}, /*index=5*/f32[2,32,256]{2,1,0:T(8,128)}) custom-call(bf16[360,256]{1,0:T(8,128)(2,1)} %get-tuple-element.16.vg_ref, bf16[360,256]{1,0:T(8,128)(2,1)} %get-tuple-element.17.gg_ref, ...), custom_call_target="tpu_custom_call" | custom-call | tf_op jit(solution)/shard_map/finish/pallas_call | solution.py:604
